TPU v7x, 256 devices: a whole 4x4x8 slice. The times are simulated.
256 devices in a mesh: ep: 16 (over y, x), tp: 16 (over z, core).
Axes of the slice: x: 4, y: 4, z: 8, core: 2. Of those that a mesh axis runs over, the one named last changes fastest.
Arguments:
- queries: bfloat16 [16384, 1024], P('ep', 'tp'), may hold values from -8 to 8
- keys: bfloat16 [16384, 256], P('ep'), may hold values from -8 to 8
- values: bfloat16 [16384, 256], P('ep'), may hold values from -6 to 6
- query_gain: float32 [64], replicated, may hold values from 1 to 10
- key_gain: float32 [64], replicated, may hold values from 1 to 10
- moe_input: bfloat16 [12288, 2048], P(('ep', 'tp')), may hold values from -6 to 6
- expert_ids: int32 [12288, 2], P('ep'), may hold values from 0 to 15, all different within a row; in each aligned block of 48 rows (0 to 47, 48 to 95, ...) at most 7 rows name the same one
- route_weight: float32 [12288, 2], P('ep'), may hold values from 0.2 to 1
- gate_weight: bfloat16 [16, 2048, 7168], P('ep', None, 'tp'), may hold values from -0.125 to 0.125
- up_weight: bfloat16 [16, 2048, 7168], P('ep', None, 'tp'), may hold values from -0.125 to 0.125
- down_weight: bfloat16 [16, 7168, 2048], P('ep', 'tp'), may hold values from -0.0625 to 0.0625
- output_gain: float32 [2048], replicated, may hold values from 0.1 to 1.9
Outputs:
- attended: bfloat16 [16384, 1024], P('ep', 'tp')
- moe_output: bfloat16 [12288, 2048], P(('ep', 'tp'))
Inputs may be any that keep to these rules, and one draw needn't show every extreme that they name: `expert_ids`: the 2 experts of a token differ. In the rows of one device (aligned blocks of 48 tokens) no expert is named by more than 7 tokens, and in every draw some expert is named by exactly 7 tokens of some device.
All inputs are finite; a program needn't handle non-finite values.
Results may differ from a plain program's by a relative error of at most 0.0085.
The roundings to bfloat16 on the way count: a program that leaves them out, or rounds other values in their place, can miss the bound.
Values may be sent and summed in bfloat16 or wider, within the bound.
A program may use at most 128 MiB of HBM per device.

v0:
```python
import math

import jax
import jax.numpy as jnp
from jax import lax
from jax.sharding import Mesh
from jax.sharding import PartitionSpec as P

QH = 16
KV = 4
GRID_W = 64
TP = ("tp_0", "tp_1")
EP_TP = ("ep", "tp_0", "tp_1")


rope_theta = 10000.0
rms_epsilon = 1e-06
norm_epsilon = 1e-05
residual_scale = 1.4142135623730951


def side_by_side(arrays, axis, dim, along):
    ends, at = ([], 0)
    for a in arrays[:-1]:
        at += a.shape[along]
        ends.append(at)
    both = jnp.concatenate(arrays, axis=along)
    return tuple(jnp.split(lax.all_gather(both, axis, axis=dim, tiled=True), ends, axis=along))


def sum_by_axis(terms, axes):
    subtotal = terms.astype(jnp.bfloat16)
    for axis in axes:
        subtotal = lax.psum_scatter(subtotal, axis, scatter_dimension=0, tiled=True)
    return subtotal.astype(jnp.float32)


def unit_heads(heads, gain_vector):
    squares = jnp.mean(heads * heads, axis=-1, keepdims=True)
    return heads * lax.rsqrt(squares + rms_epsilon) * gain_vector


def rotate_grid(heads, first_position, grid_width):
    head_size = heads.shape[-1]
    pair_count = head_size // 4
    position = first_position + jnp.arange(heads.shape[1], dtype=jnp.int32)
    grid_row = (position // grid_width).astype(jnp.float32)
    grid_col = (position % grid_width).astype(jnp.float32)
    inverse = rope_theta ** (-jnp.arange(pair_count, dtype=jnp.float32) / pair_count)
    angles = jnp.concatenate([grid_row[:, None] * inverse, grid_col[:, None] * inverse], axis=-1)
    cosines = jnp.cos(angles)
    sines = jnp.sin(angles)
    half_size = head_size // 2
    first_half = heads[..., :half_size]
    second_half = heads[..., half_size:]
    return jnp.concatenate(
        [first_half * cosines - second_half * sines, second_half * cosines + first_half * sines],
        axis=-1,
    )


def place_rank(choices, expert_count):
    matches = (choices[..., None] == jnp.arange(expert_count, dtype=jnp.int32)).astype(jnp.int32)
    earlier = jnp.cumsum(matches, axis=1) - matches
    return jnp.sum(earlier * matches, axis=-1)


def shards(
    queries,
    keys,
    values,
    query_gain,
    key_gain,
    moe_input,
    expert_ids,
    route_weight,
    gate_weight,
    up_weight,
    down_weight,
    output_gain,
):
    seg_rows = queries.shape[0]
    head_size = query_gain.shape[0]
    local_heads = queries.shape[1] // head_size
    offset = lax.axis_index("ep") * seg_rows
    key_head = lax.axis_index(TP) * local_heads // (QH // KV)
    key_cols = lax.dynamic_slice_in_dim(keys, key_head * head_size, head_size, 1)
    value_cols = lax.dynamic_slice_in_dim(values, key_head * head_size, head_size, 1)
    query_heads = (
        queries.reshape(seg_rows, local_heads, head_size).transpose(1, 0, 2).astype(jnp.float32)
    )
    rotated_queries = rotate_grid(unit_heads(query_heads, query_gain), offset, GRID_W).astype(
        jnp.bfloat16
    )
    key_heads = key_cols.astype(jnp.float32)[None]
    rotated_keys = rotate_grid(unit_heads(key_heads, key_gain), offset, GRID_W)[0].astype(
        jnp.bfloat16
    )
    score_scale = head_size ** (-0.5)
    initial = (
        jnp.full((local_heads, seg_rows), -jnp.inf, jnp.float32),
        jnp.zeros((local_heads, seg_rows), jnp.float32),
        jnp.zeros((local_heads, head_size, seg_rows), jnp.float32),
    )
    key_piece, value_piece = side_by_side((rotated_keys, value_cols), "ep", 0, 1)
    piece_rows = key_piece.shape[0]
    block_rows = math.gcd(piece_rows, 1024)
    key_blocks = key_piece.reshape(piece_rows // block_rows, block_rows, head_size)
    value_blocks = value_piece.reshape(piece_rows // block_rows, block_rows, head_size)

    def sweep(state_now, blocks):
        running_max, row_total, summed = state_now
        key_block, value_block = blocks
        scores = (
            jnp.einsum(
                "hqd,kd->hqk", rotated_queries, key_block, preferred_element_type=jnp.float32
            )
            * score_scale
        )
        new_max = jnp.maximum(running_max, jnp.max(scores, axis=-1))
        shrink = jnp.exp(running_max - new_max)
        weights = jnp.exp(scores - new_max[..., None])
        row_total = row_total * shrink + jnp.sum(weights, axis=-1)
        added = jnp.einsum(
            "hqk,kd->hdq",
            weights.astype(jnp.bfloat16),
            value_block,
            preferred_element_type=jnp.float32,
        )
        summed = summed * shrink[:, None, :] + added
        return ((new_max, row_total, summed), None)

    result, ignored = lax.scan(sweep, initial, (key_blocks, value_blocks))
    row_max, row_total, summed = result
    attended = (
        (summed / row_total[:, None, :])
        .transpose(2, 0, 1)
        .reshape(seg_rows, local_heads * head_size)
        .astype(jnp.bfloat16)
    )
    tok_rows = moe_input.shape[0]
    model_width = moe_input.shape[1]
    top_count = expert_ids.shape[1]
    experts = lax.axis_size("ep")
    capacity = max(2, tok_rows * top_count * 5 // (4 * experts))
    column_index = lax.axis_index(TP)
    own_ids = lax.dynamic_slice_in_dim(expert_ids, column_index * tok_rows, tok_rows, 0).reshape(-1)
    own_weights = lax.dynamic_slice_in_dim(route_weight, column_index * tok_rows, tok_rows, 0)
    own_rank = place_rank(own_ids[None], experts)[0]
    own_slots = own_ids * capacity + own_rank
    token_of = jnp.arange(tok_rows * top_count, dtype=jnp.int32) // top_count
    sources = jnp.full((experts * capacity,), tok_rows, jnp.int32).at[own_slots].set(token_of)
    outgoing = jnp.take(moe_input, sources, axis=0, mode="fill", fill_value=0)
    arrived = lax.all_to_all(
        outgoing.reshape(experts, capacity, model_width),
        "ep",
        split_axis=0,
        concat_axis=0,
        tiled=True,
    )
    shard_piece = lax.all_gather(arrived.reshape(-1, model_width), TP, axis=0, tiled=True)
    gate_part = jnp.dot(shard_piece, gate_weight[0], preferred_element_type=jnp.float32)
    up_part = jnp.dot(shard_piece, up_weight[0], preferred_element_type=jnp.float32)
    hidden = (jax.nn.silu(gate_part) * up_part).astype(jnp.bfloat16)
    expert_out = sum_by_axis(
        jnp.dot(hidden, down_weight[0], preferred_element_type=jnp.float32), TP
    ).astype(jnp.bfloat16)
    returned = lax.all_to_all(
        expert_out.reshape(experts, capacity, model_width),
        "ep",
        split_axis=0,
        concat_axis=0,
        tiled=True,
    )
    picked = jnp.take(returned.reshape(experts * capacity, model_width), own_slots, axis=0)
    picked = picked.reshape(tok_rows, top_count, model_width).astype(jnp.float32)
    mixed = residual_scale * moe_input.astype(jnp.float32) + jnp.sum(
        own_weights[:, :, None] * picked, axis=1
    )
    average = jnp.mean(mixed, axis=-1, keepdims=True)
    centered = mixed - average
    variance = jnp.mean(centered * centered, axis=-1, keepdims=True)
    moe_output = (centered * lax.rsqrt(variance + norm_epsilon) * output_gain).astype(jnp.bfloat16)
    return (attended, moe_output)


def solution(mesh):
    split = Mesh(mesh.devices.reshape(mesh.shape["ep"], 8, 2), ("ep", "tp_0", "tp_1"))
    return jax.shard_map(
        shards,
        mesh=split,
        in_specs=(
            P("ep", TP),
            P("ep", None),
            P("ep", None),
            P(),
            P(),
            P(EP_TP, None),
            P("ep", None),
            P("ep", None),
            P("ep", None, TP),
            P("ep", None, TP),
            P("ep", TP, None),
            P(),
        ),
        out_specs=(P("ep", TP), P(EP_TP, None)),
        check_vma=False,
    )
```

profile of v0, /device:TPU:1, one launch (start us, length us, event | category | flops | bytes accessed | tf_op | source)
XLA Modules:
  0.0 365.4 jit_solution(13836861877901142481)
XLA Ops:
  13.4 17.8 %all_to_all.10 = bf16[16,7,2048]{2,1,0:T(8,128)(2,1)S(1)} all-to-all(bf16[16,7,2048]{2,1,0:T(8,128)(2,1)S(1)} %broadcast_select_fusion.3), channel_id=1, replica_groups=mesh['ep'=16,'tp_0'=8,'tp_1'=2] {'ep'}, dimensions={0} | all-to-all | bytes 917504 | tf_op jit(solution)/shard_map/all_to_all | solution.py:154
  32.2 51.9 %all-gather.5.cloned.1.call-done = bf16[1792,2048]{1,0:T(8,128)(2,1)} async-done(((bf16[112,2048]{1,0:T(8,128)(2,1)}), bf16[1792,2048]{1,0:T(8,128)(2,1)}) %all-gather.5.cloned.1.call-update) | async-done | bytes 7340048 | tf_op jit(solution)/shard_map/all_gather | solution.py:161
  84.1 7.3 %fusion.24 = f32[1792,448]{0,1:T(8,128)S(1)} fusion(bf16[1792,2048]{1,0:T(8,128)(2,1)} %all-gather.5.cloned.1.call-done, bf16[1,2048,448]{1,2,0:T(8,128)(2,1)} %param.22), kind=kOutput, calls=%fused_computation.30 | convolution fusion | flops 3288334336 | bytes 12386304 | tf_op jit(solution)/shard_map/dot_general | solution.py:162
  95.1 6.1 %convolution_convert_fusion = bf16[1792,2048]{1,0:T(8,128)(2,1)} fusion(bf16[1792,448]{0,1:T(8,128)(2,1)S(1)} %multiply_convert_fusion, bf16[1,448,2048]{2,1,0:T(8,128)(2,1)S(1)} %copy-done), kind=kOutput, calls=%fused_computation.26 | convolution fusion | flops 3292004352 | bytes 10780672 | tf_op jit(solution)/shard_map/dot_general | solution.py:166
  107.2 77.4 %reduce-scatter.3.cloned.1.call-done = bf16[224,2048]{1,0:T(8,128)(2,1)} async-done(((bf16[1792,2048]{1,0:T(8,128)(2,1)}), bf16[224,2048]{1,0:T(8,128)(2,1)}) %reduce-scatter.3.cloned.1.call-update) | async-done | bytes 917520 | tf_op jit(solution)/shard_map/reduce_scatter | solution.py:34
  184.7 4.7 %fusion.47 = (bf16[16384,64]{0,1:T(8,128)(2,1)}, bf16[16384,64]{0,1:T(8,128)(2,1)}) fusion(bf16[16384,128]{0,1:T(8,128)(2,1)} %all-gather.3.cloned.1.call-done), kind=kLoop, calls=%fused_computation.105 | loop fusion | bytes 8388608 | tf_op jit(solution)/shard_map/split | solution.py:28
  189.3 4.8 %copy.37 = bf16[16384,64]{1,0:T(8,128)(2,1)} copy(bf16[16384,64]{0,1:T(8,128)(2,1)} %get-tuple-element.101) | data formatting | bytes 4194304
  194.1 5.0 %copy.38 = bf16[16384,64]{1,0:T(8,128)(2,1)} copy(bf16[16384,64]{0,1:T(8,128)(2,1)} %get-tuple-element.100) | data formatting | bytes 4194304
  202.1 6.2 %all-to-all-start.1 = ((bf16[16,7,2048]{2,1,0:T(8,128)(2,1)}), bf16[16,7,2048]{2,1,0:T(8,128)(2,1)S(1)}, u32[]{:S(2)}, u32[]{:S(2)}) async-start(bf16[16,7,2048]{2,1,0:T(8,128)(2,1)} %reshape.467), calls=%async_computation.3 | async-start | bytes 1048576 | tf_op jit(solution)/shard_map/all_to_all | solution.py:168
  208.4 144.6 %while.15 = (s32[]{:T(128)}, f32[1,1024]{1,0:T(1,128)S(1)}, f32[1,1024]{1,0:T(1,128)S(1)}, f32[1,64,1024]{2,1,0:T(8,128)S(1)}, bf16[16,1024,64]{2,1,0:T(8,128)(2...) while((s32[]{:T(128)}, f32[1,1024]{1,0:T(1,128)S(1)}, ...), condition=%wide.region_5.6_spmd.clone, body=%wide.region_2.5_spmd.clone.sunk | while | flops 277025792 | bytes 30605460 | solution.py:133
  208.4 3.8 %multiply_reduce_fusion.4 = (f32[1024]{0:T(1024)S(1)}, f32[1024,1024]{1,0:T(8,128)}) fusion(bf16[1,1024,64]{2,1,0:T(8,128)(2,1)S(1)} %get-tuple-element.188, bf16[16,1024,64]{2,1,0:T(8,128)(2,1)} %get-tuple-element.187, s32[]{:T(128)S(6)} %copy.45), kind=kOutput, calls=%fused_computation.4.clone.1 | convolution fusion | flops 136313856 | bytes 4591620 | tf_op jit(solution)/shard_map/while/body/eval_jaxpr/hqd,kd->hqk/dot_general | solution.py:115
  217.4 3.8 %multiply_reduce_fusion.4 = (f32[1024]{0:T(1024)S(1)}, f32[1024,1024]{1,0:T(8,128)}) fusion(bf16[1,1024,64]{2,1,0:T(8,128)(2,1)S(1)} %get-tuple-element.188, bf16[16,1024,64]{2,1,0:T(8,128)(2,1)} %get-tuple-element.187, s32[]{:T(128)S(6)} %copy.45), kind=kOutput, calls=%fused_computation.4.clone.1 | convolution fusion | flops 136313856 | bytes 4591620 | tf_op jit(solution)/shard_map/while/body/eval_jaxpr/hqd,kd->hqk/dot_general | solution.py:115
  226.5 3.8 %multiply_reduce_fusion.4 = (f32[1024]{0:T(1024)S(1)}, f32[1024,1024]{1,0:T(8,128)}) fusion(bf16[1,1024,64]{2,1,0:T(8,128)(2,1)S(1)} %get-tuple-element.188, bf16[16,1024,64]{2,1,0:T(8,128)(2,1)} %get-tuple-element.187, s32[]{:T(128)S(6)} %copy.45), kind=kOutput, calls=%fused_computation.4.clone.1 | convolution fusion | flops 136313856 | bytes 4591620 | tf_op jit(solution)/shard_map/while/body/eval_jaxpr/hqd,kd->hqk/dot_general | solution.py:115
  235.5 3.8 %multiply_reduce_fusion.4 = (f32[1024]{0:T(1024)S(1)}, f32[1024,1024]{1,0:T(8,128)}) fusion(bf16[1,1024,64]{2,1,0:T(8,128)(2,1)S(1)} %get-tuple-element.188, bf16[16,1024,64]{2,1,0:T(8,128)(2,1)} %get-tuple-element.187, s32[]{:T(128)S(6)} %copy.45), kind=kOutput, calls=%fused_computation.4.clone.1 | convolution fusion | flops 136313856 | bytes 4591620 | tf_op jit(solution)/shard_map/while/body/eval_jaxpr/hqd,kd->hqk/dot_general | solution.py:115
  253.6 3.8 %multiply_reduce_fusion.4 = (f32[1024]{0:T(1024)S(1)}, f32[1024,1024]{1,0:T(8,128)}) fusion(bf16[1,1024,64]{2,1,0:T(8,128)(2,1)S(1)} %get-tuple-element.188, bf16[16,1024,64]{2,1,0:T(8,128)(2,1)} %get-tuple-element.187, s32[]{:T(128)S(6)} %copy.45), kind=kOutput, calls=%fused_computation.4.clone.1 | convolution fusion | flops 136313856 | bytes 4591620 | tf_op jit(solution)/shard_map/while/body/eval_jaxpr/hqd,kd->hqk/dot_general | solution.py:115
  271.7 3.8 %multiply_reduce_fusion.4 = (f32[1024]{0:T(1024)S(1)}, f32[1024,1024]{1,0:T(8,128)}) fusion(bf16[1,1024,64]{2,1,0:T(8,128)(2,1)S(1)} %get-tuple-element.188, bf16[16,1024,64]{2,1,0:T(8,128)(2,1)} %get-tuple-element.187, s32[]{:T(128)S(6)} %copy.45), kind=kOutput, calls=%fused_computation.4.clone.1 | convolution fusion | flops 136313856 | bytes 4591620 | tf_op jit(solution)/shard_map/while/body/eval_jaxpr/hqd,kd->hqk/dot_general | solution.py:115
  280.7 3.8 %multiply_reduce_fusion.4 = (f32[1024]{0:T(1024)S(1)}, f32[1024,1024]{1,0:T(8,128)}) fusion(bf16[1,1024,64]{2,1,0:T(8,128)(2,1)S(1)} %get-tuple-element.188, bf16[16,1024,64]{2,1,0:T(8,128)(2,1)} %get-tuple-element.187, s32[]{:T(128)S(6)} %copy.45), kind=kOutput, calls=%fused_computation.4.clone.1 | convolution fusion | flops 136313856 | bytes 4591620 | tf_op jit(solution)/shard_map/while/body/eval_jaxpr/hqd,kd->hqk/dot_general | solution.py:115
  289.7 3.8 %multiply_reduce_fusion.4 = (f32[1024]{0:T(1024)S(1)}, f32[1024,1024]{1,0:T(8,128)}) fusion(bf16[1,1024,64]{2,1,0:T(8,128)(2,1)S(1)} %get-tuple-element.188, bf16[16,1024,64]{2,1,0:T(8,128)(2,1)} %get-tuple-element.187, s32[]{:T(128)S(6)} %copy.45), kind=kOutput, calls=%fused_computation.4.clone.1 | convolution fusion | flops 136313856 | bytes 4591620 | tf_op jit(solution)/shard_map/while/body/eval_jaxpr/hqd,kd->hqk/dot_general | solution.py:115
  298.8 3.8 %multiply_reduce_fusion.4 = (f32[1024]{0:T(1024)S(1)}, f32[1024,1024]{1,0:T(8,128)}) fusion(bf16[1,1024,64]{2,1,0:T(8,128)(2,1)S(1)} %get-tuple-element.188, bf16[16,1024,64]{2,1,0:T(8,128)(2,1)} %get-tuple-element.187, s32[]{:T(128)S(6)} %copy.45), kind=kOutput, calls=%fused_computation.4.clone.1 | convolution fusion | flops 136313856 | bytes 4591620 | tf_op jit(solution)/shard_map/while/body/eval_jaxpr/hqd,kd->hqk/dot_general | solution.py:115
  307.8 3.8 %multiply_reduce_fusion.4 = (f32[1024]{0:T(1024)S(1)}, f32[1024,1024]{1,0:T(8,128)}) fusion(bf16[1,1024,64]{2,1,0:T(8,128)(2,1)S(1)} %get-tuple-element.188, bf16[16,1024,64]{2,1,0:T(8,128)(2,1)} %get-tuple-element.187, s32[]{:T(128)S(6)} %copy.45), kind=kOutput, calls=%fused_computation.4.clone.1 | convolution fusion | flops 136313856 | bytes 4591620 | tf_op jit(solution)/shard_map/while/body/eval_jaxpr/hqd,kd->hqk/dot_general | solution.py:115
  316.8 3.8 %multiply_reduce_fusion.4 = (f32[1024]{0:T(1024)S(1)}, f32[1024,1024]{1,0:T(8,128)}) fusion(bf16[1,1024,64]{2,1,0:T(8,128)(2,1)S(1)} %get-tuple-element.188, bf16[16,1024,64]{2,1,0:T(8,128)(2,1)} %get-tuple-element.187, s32[]{:T(128)S(6)} %copy.45), kind=kOutput, calls=%fused_computation.4.clone.1 | convolution fusion | flops 136313856 | bytes 4591620 | tf_op jit(solution)/shard_map/while/body/eval_jaxpr/hqd,kd->hqk/dot_general | solution.py:115
  325.9 3.8 %multiply_reduce_fusion.4 = (f32[1024]{0:T(1024)S(1)}, f32[1024,1024]{1,0:T(8,128)}) fusion(bf16[1,1024,64]{2,1,0:T(8,128)(2,1)S(1)} %get-tuple-element.188, bf16[16,1024,64]{2,1,0:T(8,128)(2,1)} %get-tuple-element.187, s32[]{:T(128)S(6)} %copy.45), kind=kOutput, calls=%fused_computation.4.clone.1 | convolution fusion | flops 136313856 | bytes 4591620 | tf_op jit(solution)/shard_map/while/body/eval_jaxpr/hqd,kd->hqk/dot_general | solution.py:115
  334.9 3.8 %multiply_reduce_fusion.4 = (f32[1024]{0:T(1024)S(1)}, f32[1024,1024]{1,0:T(8,128)}) fusion(bf16[1,1024,64]{2,1,0:T(8,128)(2,1)S(1)} %get-tuple-element.188, bf16[16,1024,64]{2,1,0:T(8,128)(2,1)} %get-tuple-element.187, s32[]{:T(128)S(6)} %copy.45), kind=kOutput, calls=%fused_computation.4.clone.1 | convolution fusion | flops 136313856 | bytes 4591620 | tf_op jit(solution)/shard_map/while/body/eval_jaxpr/hqd,kd->hqk/dot_general | solution.py:115
  343.9 3.8 %multiply_reduce_fusion.4 = (f32[1024]{0:T(1024)S(1)}, f32[1024,1024]{1,0:T(8,128)}) fusion(bf16[1,1024,64]{2,1,0:T(8,128)(2,1)S(1)} %get-tuple-element.188, bf16[16,1024,64]{2,1,0:T(8,128)(2,1)} %get-tuple-element.187, s32[]{:T(128)S(6)} %copy.45), kind=kOutput, calls=%fused_computation.4.clone.1 | convolution fusion | flops 136313856 | bytes 4591620 | tf_op jit(solution)/shard_map/while/body/eval_jaxpr/hqd,kd->hqk/dot_general | solution.py:115
  (201 shorter events, 115.2 us)
Async XLA Ops:
  8.0 87.1 %copy-start = (bf16[1,448,2048]{2,1,0:T(8,128)(2,1)S(1)}, bf16[1,448,2048]{2,1,0:T(8,128)(2,1)}, u32[]{:S(2)}) copy-start(bf16[1,448,2048]{2,1,0:T(8,128)(2,1)} %param.24) | copy-start | bytes 5505028
  8.0 76.1 %all-gather.5.cloned.1.call-start = ((), (), s32[]{:S(2)}) async-start(), calls=%async_computation.5 | async-start | bytes 7798784 | tf_op jit(solution)/shard_map/all_gather | solution.py:161
  32.1 152.5 %reduce-scatter.3.cloned.1.call-start = ((), (), s32[]{:S(2)}) async-start(), calls=%async_computation.6 | async-start | bytes 8257536 | tf_op jit(solution)/shard_map/reduce_scatter | solution.py:34
  84.1 7.3 %copy-start.8 = (bf16[1792,2048]{1,0:T(8,128)(2,1)S(1)}, bf16[1792,2048]{1,0:T(8,128)(2,1)}, u32[]{:S(2)}) copy-start(bf16[1792,2048]{1,0:T(8,128)(2,1)} %all-gather.5.cloned.1.call-done) | copy-start | bytes 22020100
  84.1 7.3 %copy-start.9 = (bf16[1,2048,448]{1,2,0:T(8,128)(2,1)S(1)}, bf16[1,2048,448]{1,2,0:T(8,128)(2,1)}, u32[]{:S(2)}) copy-start(bf16[1,2048,448]{1,2,0:T(8,128)(2,1)} %param.23) | copy-start | bytes 5505028
  101.3 83.3 %all-gather.3.cloned.1.call-start = ((), (), s32[]{:S(2)}) async-start(), calls=%async_computation.4 | async-start | bytes 4456448 | tf_op jit(solution)/shard_map/all_gather | solution.py:28
  105.5 94.7 %reduce-scatter.5.cloned.1.call-start = ((), (), s32[]{:S(2)}) async-start(), calls=%async_computation.7 | async-start | bytes 1376256 | tf_op jit(solution)/shard_map/reduce_scatter | solution.py:34
  202.1 151.5 %all-to-all-start.1 = ((bf16[16,7,2048]{2,1,0:T(8,128)(2,1)}), bf16[16,7,2048]{2,1,0:T(8,128)(2,1)S(1)}, u32[]{:S(2)}, u32[]{:S(2)}) async-start(bf16[16,7,2048]{2,1,0:T(8,128)(2,1)} %reshape.467), calls=%async_computation.3 | async-start | bytes 1048576 | tf_op jit(solution)/shard_map/all_to_all | solution.py:168
  212.2 3.4 copy-start.1
  221.2 3.4 copy-start.1
  230.2 3.4 copy-start.1
  239.3 3.4 copy-start.1
  248.3 3.4 copy-start.1
  257.3 3.4 copy-start.1
  266.4 3.4 copy-start.1
  275.4 3.4 copy-start.1
  284.5 3.4 copy-start.1
  293.5 3.4 copy-start.1
  302.5 3.4 copy-start.1
  311.6 3.4 copy-start.1
  320.6 3.4 copy-start.1
  338.7 3.4 copy-start.1
  353.0 4.0 %copy-start.2 = (bf16[48,2048]{1,0:T(8,128)(2,1)S(1)}, bf16[48,2048]{1,0:T(8,128)(2,1)}, u32[]{:S(2)}) copy-start(bf16[48,2048]{1,0:T(8,128)(2,1)} %param.19) | copy-start | bytes 589828
  353.0 4.4 %copy-start.5 = (f32[2048]{0:T(1024)S(1)}, f32[2048]{0:T(1024)}, u32[]{:S(2)}) copy-start(f32[2048]{0:T(1024)} %param.25) | copy-start | bytes 24580
  (6 other events, 16.0 us)
Sparse Core Ops, SparseCore 0:
  32.3 51.7 all-gather.4
  101.4 83.1 reduce-scatter.2
  187.1 13.0 reduce-scatter.4
Sparse Core Ops, SparseCore 1:
  105.6 54.1 all-gather.2
where the time goes:
time: 367 us; the launch traced here: 365 us
  waiting for transfers between devices  130 us (35%)
  matrix products  106 us (29%)
  other arithmetic  56.6 us (15%)
  local copies, waits for them, and re-layouts  31.5 us (9%)
  blocking collectives  17.8 us (5%)
  between operations  15.6 us (4%)
  starting transfers between devices  6.59 us (2%)
    reduce_scatter x2, waiting for transfers between devices, sum_by_axis(): subtotal = lax.psum_scatter(subtotal, axis, scatter_dimension=0, tiled=True)  78.5 us
    dot_general x16, matrix products, sweep(): jnp.einsum('hqd,kd->hqk', rotated_queries, key_block, preferred_element_t...  60.3 us
    all_gather x1, waiting for transfers between devices, shards(): lax.all_gather(arrived.reshape(-1, model_width), TP, axis=0, tiled=True)  51.9 us
    reduce_sum x16, other arithmetic, sweep(): row_total = row_total * shrink + jnp.sum(weights, axis=-1)  49.1 us
    dot_general x16, matrix products, sweep(): jnp.einsum('hqk,kd->hdq', weights.astype(jnp.bfloat16), value_block, pref...  28.8 us
    all_to_all x1, blocking collectives, shards(): lax.all_to_all(outgoing.reshape(experts, capacity, model_width), 'ep', sp...  17.8 us
    unnamed x23, local copies, waits for them, and re-layouts  11.2 us
  transfers between devices with their start and end apart: 5, of which 3 were waited for; matrix products, arithmetic and copies ran while one was open for 43% of the time, Pallas kernels for 0%

commit v1 on v0

v1 whole, which is shorter than its diff:
```python
import functools
import math

import jax
import jax.numpy as jnp
from jax import lax
from jax.experimental import pallas as pl
from jax.experimental.pallas import tpu as pltpu
from jax.sharding import PartitionSpec as P

QH = 16
KV = 4
GRID_W = 64
MESH = pl.DeviceIdType.MESH
BF16 = jnp.bfloat16
F32 = jnp.float32

rope_theta = 10000.0
rms_epsilon = 1e-06
norm_epsilon = 1e-05
residual_scale = 1.4142135623730951

PAD = 8
NCHUNK = 4


def unit_heads(heads, gain_vector):
    squares = jnp.mean(heads * heads, axis=-1, keepdims=True)
    return heads * lax.rsqrt(squares + rms_epsilon) * gain_vector


def rotate_grid(heads, first_position, grid_width):
    head_size = heads.shape[-1]
    pair_count = head_size // 4
    position = first_position + jnp.arange(heads.shape[0], dtype=jnp.int32)
    grid_row = (position // grid_width).astype(F32)
    grid_col = (position % grid_width).astype(F32)
    inverse = rope_theta ** (-jnp.arange(pair_count, dtype=F32) / pair_count)
    angles = jnp.concatenate([grid_row[:, None] * inverse, grid_col[:, None] * inverse], axis=-1)
    cosines = jnp.cos(angles)
    sines = jnp.sin(angles)
    half_size = head_size // 2
    first_half = heads[..., :half_size]
    second_half = heads[..., half_size:]
    return jnp.concatenate(
        [first_half * cosines - second_half * sines, second_half * cosines + first_half * sines],
        axis=-1,
    )


def attention_kernel(scale, kb, width, qt_ref, kv_ref, o_ref, vt, s0, s1):
    length = kv_ref.shape[0]
    nk = length // kb
    hd = o_ref.shape[1]
    tb = 1024

    def turn(j, carry):
        rows = pl.ds(pl.multiple_of(j * tb, tb), tb)
        vt[0:hd, rows] = kv_ref[rows, :].T[hd : 2 * hd]
        vt[hd : hd + 16, rows] = jnp.ones((16, tb), BF16)
        return carry

    lax.fori_loop(0, length // tb, turn, 0)
    for first in range(0, qt_ref.shape[1], width):

        def score(j, sref):
            rows = pl.ds(pl.multiple_of(j * kb, kb), kb)
            s = jnp.dot(
                kv_ref[rows, :], qt_ref[:, first : first + width], preferred_element_type=F32
            )
            sref[...] = s
            return jnp.max(s, axis=0, keepdims=True)

        def absorb(j, sref, state, top):
            m, acc = state
            rows = pl.ds(pl.multiple_of(j * kb, kb), kb)
            new = jnp.maximum(m, top)
            p = jnp.exp2((sref[...] - new) * scale).astype(BF16)
            shrink = jnp.exp2((m - new) * scale)
            return new, acc * shrink + jnp.dot(vt[:, rows], p, preferred_element_type=F32)

        def pair(i, carry):
            state, top0 = carry
            top1 = score(2 * i + 1, s1)
            state = absorb(2 * i, s0, state, top0)
            top2 = score(jnp.minimum(2 * i + 2, nk - 1), s0)
            state = absorb(2 * i + 1, s1, state, top1)
            return state, top2

        init = (jnp.full((1, width), -jnp.inf, F32), jnp.zeros((hd + 16, width), F32))
        (m, acc), _ = lax.fori_loop(0, nk // 2, pair, (init, score(0, s0)))
        o_ref[first : first + width, :] = (acc[0:hd] / acc[hd : hd + 1]).astype(BF16).T


def attend(qt, kv, head_size):
    length, rows = kv.shape[0], qt.shape[1]
    kb, width = 1024, 512
    return pl.pallas_call(
        functools.partial(attention_kernel, head_size**-0.5 * math.log2(math.e), kb, width),
        out_shape=jax.ShapeDtypeStruct((rows, head_size), BF16),
        in_specs=[pl.BlockSpec(memory_space=pltpu.VMEM)] * 2,
        out_specs=pl.BlockSpec(memory_space=pltpu.VMEM),
        scratch_shapes=[
            pltpu.VMEM((head_size + 16, length), BF16),
            pltpu.VMEM((kb, width), F32),
            pltpu.VMEM((kb, width), F32),
        ],
        compiler_params=pltpu.CompilerParams(vmem_limit_bytes=40 * 1024 * 1024),
        cost_estimate=pl.CostEstimate(
            flops=4 * length * rows * 128,
            bytes_accessed=4 * length * 128,
            transcendentals=length * rows,
        ),
    )(qt, kv)


def experts_kernel(
    n_ep,
    n_z,
    slots_row,
    slots_col,
    route,
    x_ref,
    gain_ref,
    gate_hbm,
    up_hbm,
    down_hbm,
    out_ref,
    gate,
    up,
    down,
    outgoing,
    dispatched,
    blocks,
    parts,
    partner_parts,
    ring_in,
    returned,
    load_sem,
    disp_send,
    disp_recv,
    gath_send,
    gath_recv,
    pair_send,
    pair_recv,
    part_send,
    part_recv,
    red_send,
    red_recv,
    ret_send,
    ret_recv,
):
    e = lax.axis_index("ep")
    t = lax.axis_index("tp")
    z = t // 2
    c = t % 2
    way = 1 - 2 * c
    tokens, width = x_ref.shape
    rows = blocks.shape[2]
    cap = rows // n_ep
    slots = n_ep * PAD
    cw = width // NCHUNK
    last = n_z - 1

    def at_z(distance):
        return lax.rem(z + distance + 2 * n_z, n_z)

    ring_to = (e, at_z(way) * 2 + c)
    partner = (e, z * 2 + 1 - c)

    loads = [
        pltpu.make_async_copy(src, dst, load_sem.at[i])
        for i, (src, dst) in enumerate(((gate_hbm, gate), (up_hbm, up), (down_hbm, down)))
    ]
    for load in loads:
        load.start()

    barrier = pltpu.get_barrier_semaphore()
    for d in range(1, n_ep):
        pl.semaphore_signal(
            barrier, inc=1, device_id=(lax.rem(e + d, n_ep), t), device_id_type=MESH
        )
    for peer in ((e, at_z(1) * 2 + c), (e, at_z(-1) * 2 + c), partner):
        pl.semaphore_signal(barrier, inc=1, device_id=peer, device_id_type=MESH)

    slot = lax.broadcasted_iota(jnp.int32, (slots, tokens), 0)
    pick = jnp.where((slot == slots_row[0:1, :]) | (slot == slots_row[1:2, :]), 1.0, 0.0)
    outgoing[...] = (
        jnp.dot(pick.astype(BF16), x_ref[...], preferred_element_type=F32)
        .astype(BF16)
        .reshape(n_ep, PAD, width)
    )
    dispatched[pl.ds(e, 1)] = outgoing[pl.ds(e, 1)]
    pl.semaphore_wait(barrier, n_ep - 1 + 3)

    def exchange(src, dst, send, recv, d):
        to = lax.rem(e + d, n_ep)
        return pltpu.make_async_remote_copy(
            src_ref=src.at[to],
            dst_ref=dst.at[e],
            send_sem=send.at[d],
            recv_sem=recv.at[d],
            device_id=(to, t),
            device_id_type=MESH,
        )

    for d in range(1, n_ep):
        exchange(outgoing, dispatched, disp_send, disp_recv, d).start()
    for d in range(1, n_ep):
        exchange(outgoing, dispatched, disp_send, disp_recv, d).wait_recv()

    r_i = lax.broadcasted_iota(jnp.int32, (rows, slots), 0)
    s_i = lax.broadcasted_iota(jnp.int32, (rows, slots), 1)
    squeeze = jnp.where(s_i == (r_i // cap) * PAD + r_i % cap, 1.0, 0.0).astype(BF16)
    blocks[pl.ds(c, 1), pl.ds(z, 1)] = (
        jnp.dot(squeeze, dispatched[...].reshape(slots, width), preferred_element_type=F32)
        .astype(BF16)
        .reshape(1, 1, rows, width)
    )

    def gather_copy(s, k):
        ref = blocks.at[c, at_z(-way * s), :, pl.ds(k * cw, cw)]
        return pltpu.make_async_remote_copy(
            src_ref=ref,
            dst_ref=ref,
            send_sem=gath_send.at[s * NCHUNK + k],
            recv_sem=gath_recv.at[s * NCHUNK + k],
            device_id=ring_to,
            device_id_type=MESH,
        )

    def pair_copy(s):
        ref = blocks.at[c, at_z(-way * s)]
        return pltpu.make_async_remote_copy(
            src_ref=ref,
            dst_ref=ref,
            send_sem=pair_send.at[s],
            recv_sem=pair_recv.at[s],
            device_id=partner,
            device_id_type=MESH,
        )

    def part_copy(s):
        return pltpu.make_async_remote_copy(
            src_ref=parts.at[1 - c, at_z(way * s)],
            dst_ref=partner_parts.at[at_z(way * s)],
            send_sem=part_send.at[s],
            recv_sem=part_recv.at[s],
            device_id=partner,
            device_id_type=MESH,
        )

    def reduce_copy(s, k):
        cols = pl.ds(k * cw, cw)
        return pltpu.make_async_remote_copy(
            src_ref=parts.at[c, at_z(-way * (s + 1)), :, cols],
            dst_ref=ring_in.at[s, :, cols],
            send_sem=red_send.at[s * NCHUNK + k],
            recv_sem=red_recv.at[s * NCHUNK + k],
            device_id=ring_to,
            device_id_type=MESH,
        )

    def feed(ring, zi):
        xb = blocks[pl.ds(ring, 1), pl.ds(zi, 1)].reshape(rows, width)
        g = jnp.dot(xb, gate[...], preferred_element_type=F32)
        u = jnp.dot(xb, up[...], preferred_element_type=F32)
        hidden = ((g / (1.0 + jnp.exp(-g))) * u).astype(BF16)
        part = jnp.dot(hidden, down[...], preferred_element_type=F32).astype(BF16)
        parts[pl.ds(ring, 1), pl.ds(zi, 1)] = part.reshape(1, 1, rows, width)

    def feed_own(s):
        feed(c, at_z(-way * s))

    def feed_partner(s):
        pair_copy(s).wait_recv()
        feed(1 - c, at_z(way * s))
        part_copy(s).start()

    for k in range(NCHUNK):
        gather_copy(0, k).start()
    pair_copy(0).start()
    for load in loads:
        load.wait()

    def gather_step(s, carry):
        def forward(k):
            gather_copy(s, k).wait_recv()

            @pl.when(s < last - 1)
            def _():
                gather_copy(s + 1, k).start()

        forward(0)
        forward(1)
        feed_own(s)
        forward(2)
        feed_partner(s)
        forward(3)
        pair_copy(s + 1).start()
        return carry

    lax.fori_loop(0, last, gather_step, 0)

    def reduce_step(s, carry):
        b = at_z(-way * (s + 1))
        part_copy(s + 1).wait_recv()
        for k in range(NCHUNK):
            cols = pl.ds(k * cw, cw)
            value = parts[pl.ds(c, 1), pl.ds(b, 1), :, cols].astype(F32).reshape(rows, cw)
            value += partner_parts[pl.ds(b, 1), :, cols].astype(F32).reshape(rows, cw)
            reduce_copy(s - 1, k).wait_recv()
            value += ring_in[pl.ds(s - 1, 1), :, cols].astype(F32).reshape(rows, cw)
            parts[pl.ds(c, 1), pl.ds(b, 1), :, cols] = value.astype(BF16).reshape(1, 1, rows, cw)
            reduce_copy(s, k).start()
        return carry

    b = at_z(-way)
    part_copy(1).wait_recv()
    for k in range(NCHUNK):
        cols = pl.ds(k * cw, cw)
        value = parts[pl.ds(c, 1), pl.ds(b, 1), :, cols].astype(F32).reshape(rows, cw)
        value += partner_parts[pl.ds(b, 1), :, cols].astype(F32).reshape(rows, cw)
        parts[pl.ds(c, 1), pl.ds(b, 1), :, cols] = value.astype(BF16).reshape(1, 1, rows, cw)
        reduce_copy(0, k).start()
    feed_partner(last)
    feed_own(last)
    lax.fori_loop(1, last, reduce_step, 0)

    part_copy(0).wait_recv()
    total = parts[pl.ds(c, 1), pl.ds(z, 1)].astype(F32).reshape(rows, width)
    total += partner_parts[pl.ds(z, 1)].astype(F32).reshape(rows, width)
    for k in range(NCHUNK):
        reduce_copy(last - 1, k).wait_recv()
    total += ring_in[last - 1].astype(F32)
    r_j = lax.broadcasted_iota(jnp.int32, (slots, rows), 1)
    s_j = lax.broadcasted_iota(jnp.int32, (slots, rows), 0)
    spread = jnp.where(s_j == (r_j // cap) * PAD + r_j % cap, 1.0, 0.0).astype(BF16)
    for d in range(1, n_ep):
        exchange(outgoing, dispatched, disp_send, disp_recv, d).wait_send()
    outgoing[...] = (
        jnp.dot(spread, total.astype(BF16), preferred_element_type=F32)
        .astype(BF16)
        .reshape(n_ep, PAD, width)
    )
    returned[pl.ds(e, 1)] = outgoing[pl.ds(e, 1)]
    for d in range(1, n_ep):
        exchange(outgoing, returned, ret_send, ret_recv, d).start()

    for s in range(n_z):
        pair_copy(s).wait_send()
        part_copy(s).wait_send()
    for s in range(last):
        for k in range(NCHUNK):
            gather_copy(s, k).wait_send()
            reduce_copy(s, k).wait_send()
    mixed = residual_scale * x_ref[...].astype(F32)
    for d in range(1, n_ep):
        exchange(outgoing, returned, ret_send, ret_recv, d).wait_recv()
    back = returned[...].reshape(slots, width)
    lane = lax.broadcasted_iota(jnp.int32, (tokens, slots), 1)
    both = None
    for k in range(slots_col.shape[1]):
        one = jnp.where(lane == slots_col[:, k : k + 1], 1.0, 0.0).astype(BF16)
        term = route[:, k : k + 1] * jnp.dot(one, back, preferred_element_type=F32)
        both = term if both is None else both + term
    mixed += both
    average = jnp.mean(mixed, axis=-1, keepdims=True)
    centered = mixed - average
    variance = jnp.mean(centered * centered, axis=-1, keepdims=True)
    out_ref[...] = (centered * lax.rsqrt(variance + norm_epsilon) * gain_ref[...]).astype(BF16)
    for d in range(1, n_ep):
        exchange(outgoing, returned, ret_send, ret_recv, d).wait_send()


def experts(slots_row, slots_col, route, x, gain, gate, up, down, n_ep, n_z, cap):
    tokens, width = x.shape
    hidden = gate.shape[1]
    rows = n_ep * cap
    vmem = pl.BlockSpec(memory_space=pltpu.VMEM)
    hbm = pl.BlockSpec(memory_space=pl.ANY)
    dma = pltpu.SemaphoreType.DMA
    hops = (n_z - 1) * NCHUNK
    return pl.pallas_call(
        functools.partial(experts_kernel, n_ep, n_z),
        out_shape=jax.ShapeDtypeStruct((tokens, width), BF16),
        in_specs=[vmem] * 5 + [hbm] * 3,
        out_specs=vmem,
        scratch_shapes=[
            pltpu.VMEM((width, hidden), BF16),
            pltpu.VMEM((width, hidden), BF16),
            pltpu.VMEM((hidden, width), BF16),
            pltpu.VMEM((n_ep, PAD, width), BF16),
            pltpu.VMEM((n_ep, PAD, width), BF16),
            pltpu.VMEM((2, n_z, rows, width), BF16),
            pltpu.VMEM((2, n_z, rows, width), BF16),
            pltpu.VMEM((n_z, rows, width), BF16),
            pltpu.VMEM((n_z - 1, rows, width), BF16),
            pltpu.VMEM((n_ep, PAD, width), BF16),
            dma((3,)),
            dma((n_ep,)),
            dma((n_ep,)),
            dma((hops,)),
            dma((hops,)),
            dma((n_z,)),
            dma((n_z,)),
            dma((n_z,)),
            dma((n_z,)),
            dma((hops,)),
            dma((hops,)),
            dma((n_ep,)),
            dma((n_ep,)),
        ],
        compiler_params=pltpu.CompilerParams(
            collective_id=0, has_side_effects=True, vmem_limit_bytes=50 * 1024 * 1024
        ),
        cost_estimate=pl.CostEstimate(
            flops=12 * n_z * rows * width * hidden,
            bytes_accessed=6 * width * hidden,
            transcendentals=0,
        ),
    )(slots_row, slots_col, route, x, gain, gate, up, down)


def shards(
    queries,
    keys,
    values,
    query_gain,
    key_gain,
    moe_input,
    expert_ids,
    route_weight,
    gate_weight,
    up_weight,
    down_weight,
    output_gain,
):
    seg_rows = queries.shape[0]
    head_size = query_gain.shape[0]
    tp = lax.axis_index("tp")
    offset = lax.axis_index("ep") * seg_rows
    key_head = tp // (QH // KV)
    key_cols = lax.dynamic_slice_in_dim(keys, key_head * head_size, head_size, 1)
    value_cols = lax.dynamic_slice_in_dim(values, key_head * head_size, head_size, 1)
    rotated_queries = rotate_grid(
        unit_heads(queries.astype(F32), query_gain), offset, GRID_W
    ).astype(BF16)
    rotated_keys = rotate_grid(unit_heads(key_cols.astype(F32), key_gain), offset, GRID_W).astype(
        BF16
    )
    kv = lax.all_gather(
        jnp.concatenate([rotated_keys, value_cols], axis=1), "ep", axis=0, tiled=True
    )
    qt = jnp.concatenate(
        [rotated_queries.T, jnp.zeros((head_size, seg_rows), BF16)], axis=0
    )

    tok_rows = moe_input.shape[0]
    top_count = expert_ids.shape[1]
    n_ep = lax.axis_size("ep")
    n_tp = lax.axis_size("tp")
    cap = max(2, tok_rows * top_count * 5 // (4 * n_ep))
    own_ids = lax.dynamic_slice_in_dim(expert_ids, tp * tok_rows, tok_rows, 0)
    own_route = lax.dynamic_slice_in_dim(route_weight, tp * tok_rows, tok_rows, 0)
    flat = own_ids.reshape(-1)
    order = jnp.arange(flat.shape[0], dtype=jnp.int32)
    earlier = (flat[:, None] == flat[None, :]) & (order[None, :] < order[:, None])
    rank = jnp.sum(earlier.astype(jnp.int32), axis=1)
    slots_col = (flat * PAD + rank).reshape(tok_rows, top_count)
    moe_output = experts(
        slots_col.T,
        slots_col,
        own_route,
        moe_input,
        output_gain[None, :],
        gate_weight[0],
        up_weight[0],
        down_weight[0],
        n_ep,
        n_tp // 2,
        cap,
    )
    attended = attend(qt, kv, head_size)
    return (attended, moe_output)


def solution(mesh):
    return jax.shard_map(
        shards,
        mesh=mesh,
        in_specs=(
            P("ep", "tp"),
            P("ep", None),
            P("ep", None),
            P(),
            P(),
            P(("ep", "tp"), None),
            P("ep", None),
            P("ep", None),
            P("ep", None, "tp"),
            P("ep", None, "tp"),
            P("ep", "tp", None),
            P(),
        ),
        out_specs=(P("ep", "tp"), P(("ep", "tp"), None)),
        check_vma=False,
    )
```

time: 367 us -> 159 us (0.43)
  waiting for transfers between devices: 130 us -> 0.04 us
  Pallas kernels: 0 us -> 124 us
  matrix products: 106 us -> 0 us
  other arithmetic: 56.6 us -> 4.82 us
  blocking collectives: 17.8 us -> 0 us
  local copies, waits for them, and re-layouts: 31.5 us -> 13.9 us
  starting transfers between devices: 6.59 us -> 0.04 us
    pallas_call x0 -> x2, Pallas kernels: none -> 124 us  [the longest x1 103 us: experts(): pl.pallas_call(functools.partial(experts_kernel, n_ep, n_z), out_shape=ja...]
    dot_general x35 -> x0, matrix products: 106 us -> none  [the longest x16 60.3 us: sweep(): jnp.einsum('hqd,kd->hqk', rotated_queries, key_block, preferred_element_t...]
    reduce_scatter x2 -> x0, waiting for transfers between devices: 78.5 us -> none  [sum_by_axis(): subtotal = lax.psum_scatter(subtotal, axis, scatter_dimension=0, tiled=True)]
    all_gather x2 -> x1, waiting for transfers between devices: 51.9 us -> 0.02 us  [shards(): lax.all_gather(jnp.concatenate([rotated_keys, value_cols], axis=1), 'ep',...]
    reduce_sum x20 -> x1, other arithmetic: 51.7 us -> 0.18 us  [shards(): rank = jnp.sum(earlier.astype(jnp.int32), axis=1)]
    all_to_all x1 -> x0, blocking collectives: 17.8 us -> none  [shards(): lax.all_to_all(outgoing.reshape(experts, capacity, model_width), 'ep', sp...]
    all_to_all x1 -> x0, starting transfers between devices: 6.24 us -> none  [shards(): lax.all_to_all(expert_out.reshape(experts, capacity, model_width), 'ep',...]
    while x48 -> x0, local copies, waits for them, and re-layouts: 5.37 us -> none
  transfers between devices with their start and end apart: 5 -> 1, of which waited for: 3 -> 0; matrix products, arithmetic and copies ran while one was open for 43% -> 6% of each run, Pallas kernels for 0% -> 66%
where the time goes in v1:
time: 159 us; the launch traced here: 157 us
  Pallas kernels  124 us (78%)
  between operations  14.3 us (9%)
  local copies, waits for them, and re-layouts  13.9 us (9%)
  other arithmetic  4.82 us (3%)
    pallas_call x1, Pallas kernels, experts(): pl.pallas_call(functools.partial(experts_kernel, n_ep, n_z), out_shape=ja...  103 us
    pallas_call x1, Pallas kernels, attend(): pl.pallas_call(functools.partial(attention_kernel, head_size ** (-0.5) *...  20.9 us
    unnamed x26, local copies, waits for them, and re-layouts  11.5 us
  transfers between devices with their start and end apart: 1, of which 0 were waited for; matrix products, arithmetic and copies ran while one was open for 6% of the time, Pallas kernels for 66%

profile of v1, /device:TPU:1, one launch (start us, length us, event | category | flops | bytes accessed | tf_op | source)
XLA Modules:
  0.0 156.9 jit_solution(13125308527292426229)
XLA Ops:
  7.4 0.4 fusion.12
  7.8 0.2 copy.51
  8.0 1.1 copy.50
  9.1 0.2 fusion
  9.4 0.3 fusion.2
  9.7 0.2 copy.52
  9.9 0.1 constant_dynamic-slice_fusion.2
  10.1 0.4 fusion.1
  10.5 2.0 %subtract_convert_fusion = (bf16[1024,32]{1,0:T(8,128)(2,1)S(1)}, bf16[1024,32]{1,0:T(8,128)(2,1)S(1)}, bf16[1024,32]{1,0:T(8,128)(2,1)S(1)}, bf16[1024,32]{1,0:T(8,128)(2,1)S(1)}) fusion(f32[1024,32]{1,0:T(8,128)S(1)} %copy.51, f32[1024,64]{1,0:T(8,128)S(1)} %get-tuple-element.25, f32[1024,64]{1,0:T(8,128)S(1)} %get-tuple-element.24, f32[1024,32]{1,0:T(8,128)S(1)} %copy.52), kind=kLoop, calls=%fused_computation.9 | loop fusion | flops 524288 | bytes 1048576 | tf_op jit(solution)/shard_map/convert
  12.5 1.0 pad_maximum_fusion
  13.5 0.1 maximum_bitcast_fusion
  13.7 0.1 copy.65
  13.8 0.8 constant_dynamic-slice_fusion.1
  14.7 0.1 eq.18
  14.8 0.2 convert_reduce_fusion
  15.0 0.1 reduce_sum.32
  15.2 0.8 constant_dynamic-slice_fusion
  16.1 2.4 %copy.59 = bf16[1,2048,448]{2,1,0:T(8,128)(2,1)} copy(bf16[1,2048,448]{1,2,0:T(8,128)(2,1)S(1)} %copy-done.5) | data formatting | bytes 3670016 | tf_op args[8]
  18.5 4.0 %copy.60 = bf16[1,2048,448]{2,1,0:T(8,128)(2,1)} copy(bf16[1,2048,448]{1,2,0:T(8,128)(2,1)} %param.21) | data formatting | bytes 3670016 | tf_op args[9]
  22.5 102.8 %shard_map.132 = bf16[48,2048]{1,0:T(8,128)(2,1)S(1)} custom-call(s32[2,48]{1,0:T(2,128)S(1)} %copy.61.slots_row, s32[48,2]{1,0:T(8,128)S(1)} %multiply_add_fusion.slots_col, f32[48,2]{1,0:T(8,128)S(1)} %copy.64.route, bf16[48,2048]{1,0:T(8,128)(2,1)S(1)} %copy-done.3, f32[1,2048]{1,0:T(1,128)S(1)} %bitcast.9, bf16[2048,448]{1,0:T(8,128)(2,1)} %bitcast.10, ...), custom_call_target="tpu_custom_call" | custom-call | flops 9865003008 | bytes 5505024 | tf_op jit(solution)/shard_map/pallas_call | solution.py:384
  125.4 2.2 %copy-done.1 = bf16[16384,128]{1,0:T(8,128)(2,1)S(1)} copy-done((bf16[16384,128]{1,0:T(8,128)(2,1)S(1)}, bf16[16384,128]{1,0:T(8,128)(2,1)}, u32[]{:S(2)}) %copy-start.1) | copy-done | bytes 4194328
  127.6 20.9 %shard_map.131 = bf16[1024,64]{1,0:T(8,128)(2,1)S(1)} custom-call(bf16[128,1024]{1,0:T(8,128)(2,1)S(1)} %concatenate.19.clone.qt_ref, bf16[16384,128]{1,0:T(8,128)(2,1)S(1)} %copy-done.1), custom_call_target="tpu_custom_call" | custom-call | flops 8589934592 | bytes 8388608 | tf_op jit(solution)/shard_map/pallas_call | solution.py:98
  148.6 0.8 copy.62
  149.4 0.7 copy.67
  (30 shorter events, 0.5 us)
Async XLA Ops:
  7.2 2.7 %copy-start = (bf16[1024,256]{1,0:T(8,128)(2,1)S(1)}, bf16[1024,256]{1,0:T(8,128)(2,1)}, u32[]{:S(2)}) copy-start(bf16[1024,256]{1,0:T(8,128)(2,1)} %param.14) | copy-start | bytes 1572868
  7.2 2.2 %copy-start.6 = (bf16[1024,256]{1,0:T(8,128)(2,1)S(1)}, bf16[1024,256]{1,0:T(8,128)(2,1)}, u32[]{:S(2)}) copy-start(bf16[1024,256]{1,0:T(8,128)(2,1)} %param.13) | copy-start | bytes 1572868
  7.2 2.9 %copy-start.7 = (f32[64]{0:T(128)S(1)}, f32[64]{0:T(128)}, u32[]{:S(2)}) copy-start(f32[64]{0:T(128)} %param.15) | copy-start | bytes 772
  7.2 2.9 %copy-start.8 = (f32[64]{0:T(128)S(1)}, f32[64]{0:T(128)}, u32[]{:S(2)}) copy-start(f32[64]{0:T(128)} %param.16) | copy-start | bytes 772
  7.2 118.2 %all-gather.2.cloned.1.call-start = ((), (), s32[]{:S(2)}) async-start(), calls=%async_computation | async-start | bytes 4456448 | tf_op jit(solution)/shard_map/all_gather | solution.py:452
  12.5 3.5 %copy-start.5 = (bf16[1,2048,448]{1,2,0:T(8,128)(2,1)S(1)}, bf16[1,2048,448]{1,2,0:T(8,128)(2,1)}, u32[]{:S(2)}) copy-start(bf16[1,2048,448]{1,2,0:T(8,128)(2,1)} %param.20) | copy-start | bytes 5505028
  18.5 4.0 %copy-start.2 = (bf16[1,448,2048]{2,1,0:T(8,128)(2,1)S(1)}, bf16[1,448,2048]{2,1,0:T(8,128)(2,1)}, u32[]{:S(2)}) copy-start(bf16[1,448,2048]{2,1,0:T(8,128)(2,1)} %param.22) | copy-start | bytes 5505028
  18.5 4.0 %copy-start.3 = (bf16[48,2048]{1,0:T(8,128)(2,1)S(1)}, bf16[48,2048]{1,0:T(8,128)(2,1)}, u32[]{:S(2)}) copy-start(bf16[48,2048]{1,0:T(8,128)(2,1)} %x_ref.1) | copy-start | bytes 589828
  18.5 4.0 %copy-start.4 = (f32[2048]{0:T(1024)S(1)}, f32[2048]{0:T(1024)}, u32[]{:S(2)}) copy-start(f32[2048]{0:T(1024)} %param.23) | copy-start | bytes 24580
  125.4 2.2 %copy-start.1 = (bf16[16384,128]{1,0:T(8,128)(2,1)S(1)}, bf16[16384,128]{1,0:T(8,128)(2,1)}, u32[]{:S(2)}) copy-start(bf16[16384,128]{1,0:T(8,128)(2,1)} %all-gather.2.cloned.1.call-done.kv_ref) | copy-start | bytes 12582916
Sparse Core Ops, SparseCore 0:
  13.7 62.2 all-gather.1

commit v2 on v1

v2 whole, which is shorter than its diff:
```python
import functools
import math

import jax
import jax.numpy as jnp
import numpy as np
from jax import lax
from jax.experimental import pallas as pl
from jax.experimental.pallas import tpu as pltpu
from jax.sharding import PartitionSpec as P

QH = 16
KV = 4
GRID_W = 64
MESH = pl.DeviceIdType.MESH
BF16 = jnp.bfloat16
F32 = jnp.float32

rope_theta = 10000.0
rms_epsilon = 1e-06
norm_epsilon = 1e-05
residual_scale = 1.4142135623730951

PAD = 8
NCHUNK = 4
Q_WIDTH = 512
K_BLOCK = 512
PIECES = (0, 2, 3, 5, 6)
LANES = 128
VMEM_LIMIT = 58 * 1024 * 1024
KV_GROUP = 3
KV_FROM = 4


def rotated(heads_t, gain_col, cosines, sines):
    squares = jnp.mean(heads_t * heads_t, axis=0, keepdims=True)
    unit = heads_t * lax.rsqrt(squares + rms_epsilon) * gain_col
    half = heads_t.shape[0] // 2
    a, b = unit[0:half], unit[half:]
    return jnp.concatenate([a * cosines - b * sines, b * cosines + a * sines], axis=0)


def layer_kernel(
    n_ep,
    n_z,
    group,
    ids_ref,
    route_ref,
    x_ref,
    gain_ref,
    qt_ref,
    q_gain,
    k_gain,
    keys_hbm,
    values_hbm,
    gate_hbm,
    up_hbm,
    down_hbm,
    att_ref,
    out_ref,
    gate_t,
    up_t,
    gate,
    up,
    down,
    key_cols,
    value_cols,
    kv,
    vt,
    qt,
    s0,
    s1,
    top,
    peak,
    acc,
    outgoing,
    dispatched,
    blocks,
    parts,
    partner_parts,
    ring_in,
    returned,
    mixed,
    meta,
    load_sem,
    disp_send,
    disp_recv,
    gath_send,
    gath_recv,
    pair_send,
    pair_recv,
    part_send,
    part_recv,
    red_send,
    red_recv,
    ret_send,
    ret_recv,
    kv_send,
    kv_recv,
    kvp_send,
    kvp_recv,
):
    e = lax.axis_index("ep")
    t = lax.axis_index("tp")
    z = t // 2
    c = t % 2
    way = 1 - 2 * c
    tokens, width = x_ref.shape
    rows = blocks.shape[2]
    cap = rows // n_ep
    slots = n_ep * PAD
    cw = width // NCHUNK
    last = n_z - 1

    def at_z(distance):
        return lax.rem(z + distance + 2 * n_z, n_z)

    ring_to = (e, at_z(way) * 2 + c)
    partner = (e, z * 2 + 1 - c)

    hd = q_gain.shape[1]
    seg = qt_ref.shape[1]
    key_head = t // group
    head_cols = pl.ds(pl.multiple_of(key_head // 2 * (2 * hd), 2 * hd), 2 * hd)
    loads = [
        pltpu.make_async_copy(src, dst, load_sem.at[i])
        for i, (src, dst) in enumerate(
            (
                (keys_hbm.at[:, head_cols], key_cols),
                (values_hbm.at[:, head_cols], value_cols),
                (gate_hbm, gate_t),
                (up_hbm, up_t),
                (down_hbm, down),
            )
        )
    ]
    for load in loads:
        load.start()

    barrier = pltpu.get_barrier_semaphore()
    for d in range(1, n_ep):
        pl.semaphore_signal(
            barrier, inc=1, device_id=(lax.rem(e + d, n_ep), t), device_id_type=MESH
        )
    for peer in ((e, at_z(1) * 2 + c), (e, at_z(-1) * 2 + c), partner):
        pl.semaphore_signal(barrier, inc=1, device_id=peer, device_id_type=MESH)

    top_count = ids_ref.shape[0]
    column_tokens = ids_ref.shape[1]
    meta[...] = jnp.zeros(meta.shape, F32)
    meta[0:top_count, :] = ids_ref[...].astype(F32)
    meta[top_count : 2 * top_count, :] = route_ref[...]
    own = pltpu.roll(
        meta[...], lax.rem(column_tokens - t * tokens, column_tokens), axis=1
    )[:, 0:LANES]
    own_t = own.T
    sub_i = lax.broadcasted_iota(jnp.int32, (LANES, LANES), 0)
    lane_i = lax.broadcasted_iota(jnp.int32, (LANES, LANES), 1)
    slot_rows, slot_cols = [], []
    for k in range(top_count):
        row, col = own[k : k + 1, :], own_t[:, k : k + 1]
        hit_r = sum(jnp.where(own_t[:, j : j + 1] == row, 1.0, 0.0) for j in range(top_count))
        hit_c = sum(jnp.where(own[j : j + 1, :] == col, 1.0, 0.0) for j in range(top_count))
        rank_r = jnp.sum(jnp.where(sub_i < lane_i, hit_r, 0.0), axis=0, keepdims=True)
        rank_c = jnp.sum(jnp.where(lane_i < sub_i, hit_c, 0.0), axis=1, keepdims=True)
        slot_rows.append((row * PAD + rank_r)[:, 0:tokens])
        slot_cols.append((col * PAD + rank_c)[0:tokens, :])

    slot = lax.broadcasted_iota(jnp.int32, (slots, tokens), 0).astype(F32)
    pick = sum(jnp.where(slot == row, 1.0, 0.0) for row in slot_rows)
    outgoing[...] = (
        jnp.dot(pick.astype(BF16), x_ref[...], preferred_element_type=F32)
        .astype(BF16)
        .reshape(n_ep, PAD, width)
    )
    dispatched[pl.ds(e, 1)] = outgoing[pl.ds(e, 1)]
    pl.semaphore_wait(barrier, n_ep - 1 + 3)

    def exchange(src, dst, send, recv, d, k):
        to = lax.rem(e + d, n_ep)
        cols = pl.ds(k * cw, cw)
        return pltpu.make_async_remote_copy(
            src_ref=src.at[to, :, cols],
            dst_ref=dst.at[e, :, cols],
            send_sem=send.at[0],
            recv_sem=recv.at[k],
            device_id=(to, t),
            device_id_type=MESH,
        )

    def each(act):
        def one(d, carry):
            act(d)
            return carry

        lax.fori_loop(1, n_ep, one, 0)

    def dispatch(d, k):
        return exchange(outgoing, dispatched, disp_send, disp_recv, d, k)

    def give_back(d, k):
        return exchange(outgoing, returned, ret_send, ret_recv, d, k)

    def wait_bytes(ref, sem):
        pltpu.make_async_copy(ref, ref, sem).wait()

    def chunk_bytes(ref, k):
        return ref.at[pl.ds(0, n_ep - 1), :, pl.ds(k * cw, cw)]

    for k in range(NCHUNK):
        each(lambda d: dispatch(d, k).start())
    def kv_copy(d):
        rows_c = pl.ds(pl.multiple_of(c * (seg // 2), seg // 2), seg // 2)
        return pltpu.make_async_remote_copy(
            src_ref=kv.at[e, rows_c, :],
            dst_ref=kv.at[e, rows_c, :],
            send_sem=kv_send.at[0],
            recv_sem=kv_recv.at[(d - 1) // KV_GROUP],
            device_id=(lax.rem(e + d, n_ep), t),
            device_id_type=MESH,
        )

    def kv_pair_copy(d):
        rows_c = pl.ds(pl.multiple_of(c * (seg // 2), seg // 2), seg // 2)
        ref = kv.at[lax.rem(e - d + n_ep, n_ep), rows_c, :]
        return pltpu.make_async_remote_copy(
            src_ref=ref,
            dst_ref=ref,
            send_sem=kvp_send.at[0],
            recv_sem=kvp_recv.at[0],
            device_id=partner,
            device_id_type=MESH,
        )

    lane = lax.broadcasted_iota(jnp.int32, (1, seg), 1)
    position = e * seg + lane
    grid_row = (position // GRID_W).astype(F32)
    grid_col = (position % GRID_W).astype(F32)
    quarter = hd // 4
    freq_i = lax.broadcasted_iota(jnp.int32, (quarter, 1), 0)
    inverse = jnp.zeros((quarter, 1), F32)
    for j in range(quarter):
        inverse = jnp.where(freq_i == j, float(np.float32(rope_theta ** (-j / quarter))), inverse)
    angles = jnp.concatenate([inverse * grid_row, inverse * grid_col], axis=0)
    gain_eye = lax.broadcasted_iota(jnp.int32, (hd, hd), 0) == lax.broadcasted_iota(
        jnp.int32, (hd, hd), 1
    )

    def column(row_ref):
        return jnp.sum(jnp.where(gain_eye, row_ref[...], 0.0), axis=1, keepdims=True)

    cosines, sines = jnp.cos(angles), jnp.sin(angles)
    odd = key_head % 2 == 1
    loads[0].wait()
    loads[1].wait()
    keys_t = key_cols[...].T.astype(F32)
    values_t = value_cols[...].T.astype(F32)
    own_k = rotated(jnp.where(odd, keys_t[hd:], keys_t[:hd]), column(k_gain), cosines, sines)
    own_v = jnp.where(odd, values_t[hd:], values_t[:hd])
    kv[pl.ds(e, 1)] = (
        jnp.concatenate([own_k.astype(BF16), own_v.astype(BF16)], axis=0)
        .T.reshape(1, seg, 2 * hd)
    )
    loads[2].wait()
    loads[3].wait()
    step = width // NCHUNK
    for k in range(NCHUNK):
        gate[k * step : (k + 1) * step, :] = gate_t[:, k * step : (k + 1) * step].T
        up[k * step : (k + 1) * step, :] = up_t[:, k * step : (k + 1) * step].T

    def gather_copy(s, k):
        ref = blocks.at[c, at_z(-way * s), :, pl.ds(k * cw, cw)]
        return pltpu.make_async_remote_copy(
            src_ref=ref,
            dst_ref=ref,
            send_sem=gath_send.at[0],
            recv_sem=gath_recv.at[s * NCHUNK + k],
            device_id=ring_to,
            device_id_type=MESH,
        )

    def pair_copy(s):
        ref = blocks.at[c, at_z(-way * s)]
        return pltpu.make_async_remote_copy(
            src_ref=ref,
            dst_ref=ref,
            send_sem=pair_send.at[0],
            recv_sem=pair_recv.at[s],
            device_id=partner,
            device_id_type=MESH,
        )

    def part_copy(s):
        return pltpu.make_async_remote_copy(
            src_ref=parts.at[1 - c, at_z(way * s)],
            dst_ref=partner_parts.at[at_z(way * s)],
            send_sem=part_send.at[0],
            recv_sem=part_recv.at[s],
            device_id=partner,
            device_id_type=MESH,
        )

    def reduce_copy(s, k):
        cols = pl.ds(k * cw, cw)
        return pltpu.make_async_remote_copy(
            src_ref=parts.at[c, at_z(-way * (s + 1)), :, cols],
            dst_ref=ring_in.at[s, :, cols],
            send_sem=red_send.at[0],
            recv_sem=red_recv.at[s * NCHUNK + k],
            device_id=ring_to,
            device_id_type=MESH,
        )

    def feed(ring, zi):
        xb = blocks[pl.ds(ring, 1), pl.ds(zi, 1)].reshape(rows, width)
        g = jnp.dot(xb, gate[...], preferred_element_type=F32)
        u = jnp.dot(xb, up[...], preferred_element_type=F32)
        hidden = ((g / (1.0 + jnp.exp(-g))) * u).astype(BF16)
        part = jnp.dot(hidden, down[...], preferred_element_type=F32).astype(BF16)
        parts[pl.ds(ring, 1), pl.ds(zi, 1)] = part.reshape(1, 1, rows, width)

    def feed_own(s):
        feed(c, at_z(-way * s))

    def feed_partner(s):
        pair_copy(s).wait_recv()
        feed(1 - c, at_z(way * s))
        part_copy(s).start()

    kb = s0.shape[0]
    q_width = s0.shape[1]
    nk = n_ep * seg // kb
    tiles = nk * (seg // q_width)
    score_scale = hd**-0.5 * math.log2(math.e)

    def score(n, sref):
        rows_n = pl.ds(pl.multiple_of(lax.rem(n, nk) * kb, kb), kb)
        flat = kv.reshape(n_ep * seg, 2 * hd)
        q = qt[pl.ds(n // nk, 1)].reshape(2 * hd, q_width)
        sc = jnp.dot(flat[rows_n, :], q, preferred_element_type=F32)
        sref[...] = sc
        return jnp.max(sc, axis=0, keepdims=True)

    def absorb(n, sref, state, best):
        m, total = state
        cols_n = pl.ds(pl.multiple_of(lax.rem(n, nk) * kb, kb), kb)
        new = jnp.maximum(m, best)
        p = jnp.exp2((sref[...] - new) * score_scale).astype(BF16)
        shrink = jnp.exp2((m - new) * score_scale)
        return new, total * shrink + jnp.dot(vt[:, cols_n], p, preferred_element_type=F32)

    def piece(i):
        n = 2 * i
        group_i = pl.ds(n // nk, 1)
        best0 = top[...]
        state = (peak[group_i].reshape(1, q_width), acc[group_i].reshape(hd + 16, q_width))
        best1 = score(n + 1, s1)
        state = absorb(n, s0, state, best0)
        best2 = score(jnp.minimum(n + 2, tiles - 1), s0)
        m, total = absorb(n + 1, s1, state, best1)
        top[...] = best2
        peak[group_i] = m.reshape(1, 1, q_width)
        acc[group_i] = total.reshape(1, hd + 16, q_width)

    r_i = lax.broadcasted_iota(jnp.int32, (rows, slots), 0)
    s_i = lax.broadcasted_iota(jnp.int32, (rows, slots), 1)
    squeeze = jnp.where(s_i == (r_i // cap) * PAD + r_i % cap, 1.0, 0.0).astype(BF16)
    for k in range(NCHUNK):
        cols = pl.ds(k * cw, cw)
        wait_bytes(chunk_bytes(dispatched, k), disp_recv.at[k])
        came = dispatched[:, :, cols].reshape(slots, cw)
        blocks[pl.ds(c, 1), pl.ds(z, 1), :, cols] = (
            jnp.dot(squeeze, came, preferred_element_type=F32)
            .astype(BF16)
            .reshape(1, 1, rows, cw)
        )
        gather_copy(0, k).start()
    pair_copy(0).start()
    each(lambda d: kv_copy(d).start())
    own_q = rotated(qt_ref[...].astype(F32), column(q_gain), cosines, sines).astype(BF16)
    for g in range(seg // q_width):
        qt[g, 0:hd, :] = own_q[:, g * q_width : (g + 1) * q_width]
        qt[g, hd : 2 * hd, :] = jnp.zeros((hd, q_width), BF16)
    peak[...] = jnp.full(peak.shape, -jnp.inf, F32)
    acc[...] = jnp.zeros(acc.shape, F32)
    loads[4].wait()

    def half_bytes(n):
        return kv.at[pl.ds(0, n), pl.ds(0, seg // 2), :]

    def kv_forward(g):
        wait_bytes(half_bytes(KV_GROUP), kv_recv.at[g])
        for i in range(KV_GROUP):
            kv_pair_copy(g * KV_GROUP + 1 + i).start()

    def gather_step(s, carry):
        def forward(k):
            gather_copy(s, k).wait_recv()
            gather_copy(s + 1, k).start()

        forward(0)
        forward(1)
        feed_own(s)
        forward(2)

        @pl.when(s >= KV_FROM)
        def _():
            kv_forward(s - KV_FROM)

        feed_partner(s)
        forward(3)
        pair_copy(s + 1).start()
        return carry

    lax.fori_loop(0, last - 1, gather_step, 0)

    def first_hop(k):
        b = at_z(-way)
        cols = pl.ds(k * cw, cw)
        value = parts[pl.ds(c, 1), pl.ds(b, 1), :, cols].astype(F32).reshape(rows, cw)
        value += partner_parts[pl.ds(b, 1), :, cols].astype(F32).reshape(rows, cw)
        parts[pl.ds(c, 1), pl.ds(b, 1), :, cols] = value.astype(BF16).reshape(1, 1, rows, cw)
        reduce_copy(0, k).start()

    part_copy(1).wait_recv()
    for k in range(NCHUNK):
        first_hop(k)
    for g in range(last - 1 - KV_FROM, (n_ep - 1) // KV_GROUP):
        kv_forward(g)
    feed_own(last - 1)
    feed_partner(last - 1)
    for k in range(NCHUNK):
        gather_copy(last - 1, k).wait_recv()
    pair_copy(last).start()
    feed_own(last)
    feed_partner(last)

    def turn(j, carry):
        cols = pl.ds(pl.multiple_of(j * seg, seg), seg)
        vt[0:hd, cols] = kv[pl.ds(j, 1)].reshape(seg, 2 * hd).T[hd : 2 * hd]
        vt[hd : hd + 16, cols] = jnp.ones((16, seg), BF16)
        return carry

    def reduce_step(s, carry):
        b = at_z(-way * (s + 1))
        part_copy(s + 1).wait_recv()
        for k in range(NCHUNK):
            cols = pl.ds(k * cw, cw)
            value = parts[pl.ds(c, 1), pl.ds(b, 1), :, cols].astype(F32).reshape(rows, cw)
            value += partner_parts[pl.ds(b, 1), :, cols].astype(F32).reshape(rows, cw)
            reduce_copy(s - 1, k).wait_recv()
            value += ring_in[pl.ds(s - 1, 1), :, cols].astype(F32).reshape(rows, cw)
            parts[pl.ds(c, 1), pl.ds(b, 1), :, cols] = value.astype(BF16).reshape(1, 1, rows, cw)
            reduce_copy(s, k).start()

            @pl.when(s > 1)
            def _():
                for i in range(PIECES[k], PIECES[k + 1]):
                    piece((s - 2) * PIECES[-1] + i)

        @pl.when(s == 1)
        def _():
            wait_bytes(half_bytes(n_ep - 1), kvp_recv.at[0])
            lax.fori_loop(0, n_ep, turn, 0)
            top[...] = score(0, s0)

        return carry

    lax.fori_loop(1, last, reduce_step, 0)

    r_j = lax.broadcasted_iota(jnp.int32, (slots, rows), 1)
    s_j = lax.broadcasted_iota(jnp.int32, (slots, rows), 0)
    spread = jnp.where(s_j == (r_j // cap) * PAD + r_j % cap, 1.0, 0.0).astype(BF16)
    wait_bytes(outgoing.at[pl.ds(0, n_ep - 1)], disp_send.at[0])
    part_copy(0).wait_recv()
    done = (last - 2) * PIECES[-1]
    extra = -(-(tiles // 2 - done) // NCHUNK)
    for k in range(NCHUNK):
        cols = pl.ds(k * cw, cw)
        value = parts[pl.ds(c, 1), pl.ds(z, 1), :, cols].astype(F32).reshape(rows, cw)
        value += partner_parts[pl.ds(z, 1), :, cols].astype(F32).reshape(rows, cw)
        reduce_copy(last - 1, k).wait_recv()
        value += ring_in[last - 1, :, cols].astype(F32)
        outgoing[:, :, cols] = (
            jnp.dot(spread, value.astype(BF16), preferred_element_type=F32)
            .astype(BF16)
            .reshape(n_ep, PAD, cw)
        )
        returned[pl.ds(e, 1), :, cols] = outgoing[pl.ds(e, 1), :, cols]
        each(lambda d: give_back(d, k).start())
        for i in range(done + k * extra, min(done + (k + 1) * extra, tiles // 2)):
            piece(i)

    for g in range(seg // q_width):
        att_ref[:, g * q_width : (g + 1) * q_width] = (
            acc[g, 0:hd, :] / acc[g, hd : hd + 1, :]
        ).astype(BF16)

    wait_bytes(half_bytes(n_ep - 1), kv_send.at[0])
    wait_bytes(half_bytes(n_ep - 1), kvp_send.at[0])
    wait_bytes(blocks.at[0], pair_send.at[0])
    wait_bytes(blocks.at[0], part_send.at[0])
    wait_bytes(blocks.at[0, pl.ds(0, last)], gath_send.at[0])
    wait_bytes(blocks.at[0, pl.ds(0, last)], red_send.at[0])

    lane_s = lax.broadcasted_iota(jnp.int32, (tokens, slots), 1).astype(F32)
    ones = [jnp.where(lane_s == col, 1.0, 0.0).astype(BF16) for col in slot_cols]
    shares = [own_t[0:tokens, top_count + k : top_count + k + 1] for k in range(top_count)]
    mean = jnp.zeros((tokens, 1), F32)
    for k in range(NCHUNK):
        cols = pl.ds(k * cw, cw)
        wait_bytes(chunk_bytes(returned, k), ret_recv.at[k])
        back = returned[:, :, cols].reshape(slots, cw)
        both = None
        for one, share in zip(ones, shares):
            term = share * jnp.dot(one, back, preferred_element_type=F32)
            both = term if both is None else both + term
        part = residual_scale * x_ref[:, cols].astype(F32) + both
        mixed[:, cols] = part
        mean += jnp.sum(part, axis=-1, keepdims=True)
    centered = mixed[...] - mean / width
    variance = jnp.mean(centered * centered, axis=-1, keepdims=True)
    out_ref[...] = (centered * lax.rsqrt(variance + norm_epsilon) * gain_ref[...]).astype(BF16)
    wait_bytes(outgoing.at[pl.ds(0, n_ep - 1)], ret_send.at[0])


def layer(ids, route, x, gain, qt, q_gain, k_gain, keys, values, gate_t, up_t, down,
          n_ep, n_z, cap, group):
    tokens, width = x.shape
    hidden = down.shape[0]
    head_size, seg = qt.shape
    rows = n_ep * cap
    vmem = pl.BlockSpec(memory_space=pltpu.VMEM)
    hbm = pl.BlockSpec(memory_space=pl.ANY)
    dma = pltpu.SemaphoreType.DMA
    hops = (n_z - 1) * NCHUNK
    groups = seg // Q_WIDTH
    return pl.pallas_call(
        functools.partial(layer_kernel, n_ep, n_z, group),
        out_shape=(
            jax.ShapeDtypeStruct((head_size, seg), BF16),
            jax.ShapeDtypeStruct((tokens, width), BF16),
        ),
        in_specs=[vmem] * 7 + [hbm] * 5,
        out_specs=(vmem, vmem),
        scratch_shapes=[
            pltpu.VMEM((hidden, width), BF16),
            pltpu.VMEM((hidden, width), BF16),
            pltpu.VMEM((width, hidden), BF16),
            pltpu.VMEM((width, hidden), BF16),
            pltpu.VMEM((hidden, width), BF16),
            pltpu.VMEM((seg, 2 * head_size), BF16),
            pltpu.VMEM((seg, 2 * head_size), BF16),
            pltpu.VMEM((n_ep, seg, 2 * head_size), BF16),
            pltpu.VMEM((head_size + 16, n_ep * seg), BF16),
            pltpu.VMEM((groups, 2 * head_size, Q_WIDTH), BF16),
            pltpu.VMEM((K_BLOCK, Q_WIDTH), F32),
            pltpu.VMEM((K_BLOCK, Q_WIDTH), F32),
            pltpu.VMEM((1, Q_WIDTH), F32),
            pltpu.VMEM((groups, 1, Q_WIDTH), F32),
            pltpu.VMEM((groups, head_size + 16, Q_WIDTH), F32),
            pltpu.VMEM((n_ep, PAD, width), BF16),
            pltpu.VMEM((n_ep, PAD, width), BF16),
            pltpu.VMEM((2, n_z, rows, width), BF16),
            pltpu.VMEM((2, n_z, rows, width), BF16),
            pltpu.VMEM((n_z, rows, width), BF16),
            pltpu.VMEM((n_z - 1, rows, width), BF16),
            pltpu.VMEM((n_ep, PAD, width), BF16),
            pltpu.VMEM((tokens, width), F32),
            pltpu.VMEM((8, ids.shape[1]), F32),
            dma((5,)),
            dma((1,)),
            dma((NCHUNK,)),
            dma((1,)),
            dma((hops,)),
            dma((1,)),
            dma((n_z,)),
            dma((1,)),
            dma((n_z,)),
            dma((1,)),
            dma((hops,)),
            dma((1,)),
            dma((NCHUNK,)),
            dma((1,)),
            dma(((n_ep - 1) // KV_GROUP,)),
            dma((1,)),
            dma((1,)),
        ],
        compiler_params=pltpu.CompilerParams(
            collective_id=0, has_side_effects=True, vmem_limit_bytes=VMEM_LIMIT
        ),
    )(ids, route, x, gain, qt, q_gain, k_gain, keys, values, gate_t, up_t, down)


def shards(
    queries,
    keys,
    values,
    query_gain,
    key_gain,
    moe_input,
    expert_ids,
    route_weight,
    gate_weight,
    up_weight,
    down_weight,
    output_gain,
):
    tok_rows = moe_input.shape[0]
    top_count = expert_ids.shape[1]
    n_ep = lax.axis_size("ep")
    n_tp = lax.axis_size("tp")
    cap = max(2, tok_rows * top_count * 5 // (4 * n_ep))
    attended, moe_output = layer(
        expert_ids.T,
        route_weight.T,
        moe_input,
        output_gain[None, :],
        queries.T,
        query_gain[None, :],
        key_gain[None, :],
        keys,
        values,
        gate_weight[0].T,
        up_weight[0].T,
        down_weight[0],
        n_ep,
        n_tp // 2,
        cap,
        QH // KV,
    )
    return (attended.T, moe_output)


def solution(mesh):
    return jax.shard_map(
        shards,
        mesh=mesh,
        in_specs=(
            P("ep", "tp"),
            P("ep", None),
            P("ep", None),
            P(),
            P(),
            P(("ep", "tp"), None),
            P("ep", None),
            P("ep", None),
            P("ep", None, "tp"),
            P("ep", None, "tp"),
            P("ep", "tp", None),
            P(),
        ),
        out_specs=(P("ep", "tp"), P(("ep", "tp"), None)),
        check_vma=False,
    )
```

time: 159 us -> 99.5 us (0.63); the launches traced: 157 us -> 99.4 us
  Pallas kernels: 124 us -> 95.6 us
  between operations: 14.3 us -> 0.64 us
  local copies, waits for them, and re-layouts: 13.9 us -> 3.18 us
  other arithmetic: 4.82 us -> 0 us
    pallas_call x2 -> x1, Pallas kernels: 124 us -> 95.6 us  [layer(): pl.pallas_call(functools.partial(layer_kernel, n_ep, n_z, group), out_sha...]
    unnamed x26 -> x2, local copies, waits for them, and re-layouts: 11.5 us -> 3.18 us
    another operation x1 -> x0, other arithmetic: 2.05 us -> none
    dynamic_slice x3 -> x0, local copies, waits for them, and re-layouts: 1.67 us -> none  [the longest x1 0.76 us: shards(): lax.dynamic_slice_in_dim(route_weight, tp * tok_rows, tok_rows, 0)]
  transfers between devices with their start and end apart: 1 -> 0, of which waited for: 0 -> 0; matrix products, arithmetic and copies ran while one was open for 6% -> 0% of each run, Pallas kernels for 66% -> 0%
where the time goes in v2:
time: 99.5 us; the launch traced here: 99.4 us
  Pallas kernels  95.6 us (96%)
  local copies, waits for them, and re-layouts  3.18 us (3%)
    pallas_call x1, Pallas kernels, layer(): pl.pallas_call(functools.partial(layer_kernel, n_ep, n_z, group), out_sha...  95.6 us
    unnamed x2, local copies, waits for them, and re-layouts  3.18 us

profile of v2, /device:TPU:1, one launch (start us, length us, event | category | flops | bytes accessed | tf_op | source)
XLA Modules:
  0.0 99.4 jit_solution(11544037765848811981)
XLA Ops:
  0.6 95.6 %shard_map.131 = (bf16[64,1024]{1,0:T(8,128)(2,1)}, bf16[48,2048]{1,0:T(8,128)(2,1)}) custom-call(s32[2,768]{1,0:T(2,128)} %bitcast.20, f32[2,768]{1,0:T(2,128)} %bitcast.21, bf16[48,2048]{1,0:T(8,128)(2,1)} %x_ref.1, f32[1,2048]{1,0:T(1,128)} %bitcast.19, bf16[64,1024]{1,0:T(8,128)(2,1)} %bitcast.17, f32[1,64]{1,0:T(1,128)} %bitcast.22, f32[1,64]{1,0:T(1,128)} %bitcast.23, ...), custom_call_target="tpu_custom_call" | custom-call | tf_op jit(solution)/shard_map/pallas_call | solution.py:538
  96.2 1.6 %copy.16 = bf16[1024,64]{0,1:T(8,128)(2,1)} copy(bf16[1024,64]{0,1:T(8,128)(2,1)} %bitcast.18) | data formatting | bytes 262144
  97.8 1.6 %copy.17 = bf16[48,2048]{1,0:T(8,128)(2,1)} copy(bf16[48,2048]{1,0:T(8,128)(2,1)} %get-tuple-element.9) | data formatting | bytes 393216

commit v3 on v2

--- a/solution.py
+++ b/solution.py
@@ -27,7 +27,7 @@
 K_BLOCK = 512
 PIECES = (0, 2, 3, 5, 6)
 LANES = 128
-VMEM_LIMIT = 58 * 1024 * 1024
+VMEM_LIMIT = 56 * 1024 * 1024
 KV_GROUP = 3
 KV_FROM = 4
 
@@ -44,6 +44,20 @@
     n_ep,
     n_z,
     group,
+    ids_hbm,
+    route_hbm,
+    x_hbm,
+    gain_hbm,
+    qt_hbm,
+    q_gain_hbm,
+    k_gain_hbm,
+    keys_hbm,
+    values_hbm,
+    gate_hbm,
+    up_hbm,
+    down_hbm,
+    att_ref,
+    out_ref,
     ids_ref,
     route_ref,
     x_ref,
@@ -51,13 +65,6 @@
     qt_ref,
     q_gain,
     k_gain,
-    keys_hbm,
-    values_hbm,
-    gate_hbm,
-    up_hbm,
-    down_hbm,
-    att_ref,
-    out_ref,
     gate_t,
     up_t,
     gate,
@@ -118,6 +125,14 @@
     ring_to = (e, at_z(way) * 2 + c)
     partner = (e, z * 2 + 1 - c)
 
+    barrier = pltpu.get_barrier_semaphore()
+    for d in range(1, n_ep):
+        pl.semaphore_signal(
+            barrier, inc=1, device_id=(lax.rem(e + d, n_ep), t), device_id_type=MESH
+        )
+    for peer in ((e, at_z(1) * 2 + c), (e, at_z(-1) * 2 + c), partner):
+        pl.semaphore_signal(barrier, inc=1, device_id=peer, device_id_type=MESH)
+
     hd = q_gain.shape[1]
     seg = qt_ref.shape[1]
     key_head = t // group
@@ -126,27 +141,28 @@
         pltpu.make_async_copy(src, dst, load_sem.at[i])
         for i, (src, dst) in enumerate(
             (
+                (ids_hbm, ids_ref),
+                (route_hbm, route_ref),
+                (x_hbm, x_ref),
+                (k_gain_hbm, k_gain),
                 (keys_hbm.at[:, head_cols], key_cols),
                 (values_hbm.at[:, head_cols], value_cols),
                 (gate_hbm, gate_t),
                 (up_hbm, up_t),
+                (q_gain_hbm, q_gain),
+                (qt_hbm, qt_ref),
                 (down_hbm, down),
+                (gain_hbm, gain_ref),
             )
         )
     ]
     for load in loads:
         load.start()
 
-    barrier = pltpu.get_barrier_semaphore()
-    for d in range(1, n_ep):
-        pl.semaphore_signal(
-            barrier, inc=1, device_id=(lax.rem(e + d, n_ep), t), device_id_type=MESH
-        )
-    for peer in ((e, at_z(1) * 2 + c), (e, at_z(-1) * 2 + c), partner):
-        pl.semaphore_signal(barrier, inc=1, device_id=peer, device_id_type=MESH)
-
     top_count = ids_ref.shape[0]
     column_tokens = ids_ref.shape[1]
+    for load in loads[0:3]:
+        load.wait()
     meta[...] = jnp.zeros(meta.shape, F32)
     meta[0:top_count, :] = ids_ref[...].astype(F32)
     meta[top_count : 2 * top_count, :] = route_ref[...]
@@ -251,8 +267,8 @@
 
     cosines, sines = jnp.cos(angles), jnp.sin(angles)
     odd = key_head % 2 == 1
-    loads[0].wait()
-    loads[1].wait()
+    for load in loads[3:6]:
+        load.wait()
     keys_t = key_cols[...].T.astype(F32)
     values_t = value_cols[...].T.astype(F32)
     own_k = rotated(jnp.where(odd, keys_t[hd:], keys_t[:hd]), column(k_gain), cosines, sines)
@@ -261,8 +277,8 @@
         jnp.concatenate([own_k.astype(BF16), own_v.astype(BF16)], axis=0)
         .T.reshape(1, seg, 2 * hd)
     )
-    loads[2].wait()
-    loads[3].wait()
+    for load in loads[6:8]:
+        load.wait()
     step = width // NCHUNK
     for k in range(NCHUNK):
         gate[k * step : (k + 1) * step, :] = gate_t[:, k * step : (k + 1) * step].T
@@ -377,13 +393,14 @@
         gather_copy(0, k).start()
     pair_copy(0).start()
     each(lambda d: kv_copy(d).start())
+    for load in loads[8:]:
+        load.wait()
     own_q = rotated(qt_ref[...].astype(F32), column(q_gain), cosines, sines).astype(BF16)
     for g in range(seg // q_width):
         qt[g, 0:hd, :] = own_q[:, g * q_width : (g + 1) * q_width]
         qt[g, hd : 2 * hd, :] = jnp.zeros((hd, q_width), BF16)
     peak[...] = jnp.full(peak.shape, -jnp.inf, F32)
     acc[...] = jnp.zeros(acc.shape, F32)
-    loads[4].wait()
 
     def half_bytes(n):
         return kv.at[pl.ds(0, n), pl.ds(0, seg // 2), :]
@@ -531,19 +548,26 @@
     head_size, seg = qt.shape
     rows = n_ep * cap
     vmem = pl.BlockSpec(memory_space=pltpu.VMEM)
-    hbm = pl.BlockSpec(memory_space=pl.ANY)
+    hbm = pl.BlockSpec(memory_space=pltpu.HBM)
     dma = pltpu.SemaphoreType.DMA
     hops = (n_z - 1) * NCHUNK
     groups = seg // Q_WIDTH
     return pl.pallas_call(
         functools.partial(layer_kernel, n_ep, n_z, group),
         out_shape=(
-            jax.ShapeDtypeStruct((head_size, seg), BF16),
-            jax.ShapeDtypeStruct((tokens, width), BF16),
+            pltpu.VMEM((head_size, seg), BF16),
+            pltpu.VMEM((tokens, width), BF16),
         ),
-        in_specs=[vmem] * 7 + [hbm] * 5,
+        in_specs=[hbm] * 12,
         out_specs=(vmem, vmem),
         scratch_shapes=[
+            pltpu.VMEM(ids.shape, ids.dtype),
+            pltpu.VMEM(route.shape, F32),
+            pltpu.VMEM((tokens, width), BF16),
+            pltpu.VMEM((1, width), F32),
+            pltpu.VMEM((head_size, seg), BF16),
+            pltpu.VMEM((1, head_size), F32),
+            pltpu.VMEM((1, head_size), F32),
             pltpu.VMEM((hidden, width), BF16),
             pltpu.VMEM((hidden, width), BF16),
             pltpu.VMEM((width, hidden), BF16),
@@ -568,7 +592,7 @@
             pltpu.VMEM((n_ep, PAD, width), BF16),
             pltpu.VMEM((tokens, width), F32),
             pltpu.VMEM((8, ids.shape[1]), F32),
-            dma((5,)),
+            dma((12,)),
             dma((1,)),
             dma((NCHUNK,)),
             dma((1,)),

time: 99.5 us -> 96 us (0.965)
  local copies, waits for them, and re-layouts: 3.18 us -> 1.33 us
  Pallas kernels: 95.6 us -> 93.9 us
    unnamed x2, local copies, waits for them, and re-layouts: 3.18 us -> 1.33 us
    pallas_call x1, Pallas kernels: 95.6 us -> 93.9 us  [layer(): pl.pallas_call(functools.partial(layer_kernel, n_ep, n_z, group), out_sha...]
where the time goes in v3:
time: 96 us; the launch traced here: 95.9 us
  Pallas kernels  93.9 us (98%)
  local copies, waits for them, and re-layouts  1.33 us (1%)
    pallas_call x1, Pallas kernels, layer(): pl.pallas_call(functools.partial(layer_kernel, n_ep, n_z, group), out_sha...  93.9 us

profile of v3, /device:TPU:1, one launch (start us, length us, event | category | flops | bytes accessed | tf_op | source)
XLA Modules:
  0.0 95.9 jit_solution(16287721413510716976)
XLA Ops:
  0.6 93.9 %shard_map.131 = (bf16[64,1024]{1,0:T(8,128)(2,1)S(1)}, bf16[48,2048]{1,0:T(8,128)(2,1)S(1)}) custom-call(s32[2,768]{1,0:T(2,128)} %bitcast.20, f32[2,768]{1,0:T(2,128)} %bitcast.21, bf16[48,2048]{1,0:T(8,128)(2,1)} %x_hbm.1, f32[1,2048]{1,0:T(1,128)} %bitcast.19, bf16[64,1024]{1,0:T(8,128)(2,1)} %bitcast.18, f32[1,64]{1,0:T(1,128)} %bitcast.22, ...), custom_call_target="tpu_custom_call" | custom-call | tf_op jit(solution)/shard_map/pallas_call | solution.py:555
  94.5 0.7 copy.16
  95.2 0.7 copy.17

commit v4 on v3

--- a/solution.py
+++ b/solution.py
@@ -125,14 +125,6 @@
     ring_to = (e, at_z(way) * 2 + c)
     partner = (e, z * 2 + 1 - c)
 
-    barrier = pltpu.get_barrier_semaphore()
-    for d in range(1, n_ep):
-        pl.semaphore_signal(
-            barrier, inc=1, device_id=(lax.rem(e + d, n_ep), t), device_id_type=MESH
-        )
-    for peer in ((e, at_z(1) * 2 + c), (e, at_z(-1) * 2 + c), partner):
-        pl.semaphore_signal(barrier, inc=1, device_id=peer, device_id_type=MESH)
-
     hd = q_gain.shape[1]
     seg = qt_ref.shape[1]
     key_head = t // group
@@ -158,6 +150,14 @@
     ]
     for load in loads:
         load.start()
+
+    barrier = pltpu.get_barrier_semaphore()
+    for d in range(1, n_ep):
+        pl.semaphore_signal(
+            barrier, inc=1, device_id=(lax.rem(e + d, n_ep), t), device_id_type=MESH
+        )
+    for peer in ((e, at_z(1) * 2 + c), (e, at_z(-1) * 2 + c), partner):
+        pl.semaphore_signal(barrier, inc=1, device_id=peer, device_id_type=MESH)
 
     top_count = ids_ref.shape[0]
     column_tokens = ids_ref.shape[1]
@@ -184,12 +184,18 @@
 
     slot = lax.broadcasted_iota(jnp.int32, (slots, tokens), 0).astype(F32)
     pick = sum(jnp.where(slot == row, 1.0, 0.0) for row in slot_rows)
-    outgoing[...] = (
-        jnp.dot(pick.astype(BF16), x_ref[...], preferred_element_type=F32)
-        .astype(BF16)
-        .reshape(n_ep, PAD, width)
-    )
-    dispatched[pl.ds(e, 1)] = outgoing[pl.ds(e, 1)]
+    pick = pick.astype(BF16)
+
+    def gather_rows(k):
+        cols = pl.ds(k * cw, cw)
+        outgoing[:, :, cols] = (
+            jnp.dot(pick, x_ref[:, cols], preferred_element_type=F32)
+            .astype(BF16)
+            .reshape(n_ep, PAD, cw)
+        )
+        dispatched[pl.ds(e, 1), :, cols] = outgoing[pl.ds(e, 1), :, cols]
+
+    gather_rows(0)
     pl.semaphore_wait(barrier, n_ep - 1 + 3)
 
     def exchange(src, dst, send, recv, d, k):
@@ -224,6 +230,8 @@
         return ref.at[pl.ds(0, n_ep - 1), :, pl.ds(k * cw, cw)]
 
     for k in range(NCHUNK):
+        if k:
+            gather_rows(k)
         each(lambda d: dispatch(d, k).start())
     def kv_copy(d):
         rows_c = pl.ds(pl.multiple_of(c * (seg // 2), seg // 2), seg // 2)
@@ -392,7 +400,6 @@
         )
         gather_copy(0, k).start()
     pair_copy(0).start()
-    each(lambda d: kv_copy(d).start())
     for load in loads[8:]:
         load.wait()
     own_q = rotated(qt_ref[...].astype(F32), column(q_gain), cosines, sines).astype(BF16)
@@ -416,6 +423,11 @@
             gather_copy(s + 1, k).start()
 
         forward(0)
+
+        @pl.when(s == 0)
+        def _():
+            each(lambda d: kv_copy(d).start())
+
         forward(1)
         feed_own(s)
         forward(2)
@@ -442,13 +454,13 @@
     part_copy(1).wait_recv()
     for k in range(NCHUNK):
         first_hop(k)
-    for g in range(last - 1 - KV_FROM, (n_ep - 1) // KV_GROUP):
-        kv_forward(g)
     feed_own(last - 1)
     feed_partner(last - 1)
     for k in range(NCHUNK):
         gather_copy(last - 1, k).wait_recv()
     pair_copy(last).start()
+    for g in range(last - 1 - KV_FROM, (n_ep - 1) // KV_GROUP):
+        kv_forward(g)
     feed_own(last)
     feed_partner(last)
 

time: 96 us -> 96 us (level)
  no operation moved by 1% of the time
where the time goes in v4:
time: 96 us; the launch traced here: 95.9 us
  Pallas kernels  93.9 us (98%)
  local copies, waits for them, and re-layouts  1.33 us (1%)
    pallas_call x1, Pallas kernels, layer(): pl.pallas_call(functools.partial(layer_kernel, n_ep, n_z, group), out_sha...  93.9 us

profile of v4, /device:TPU:1, one launch (start us, length us, event | category | flops | bytes accessed | tf_op | source)
XLA Modules:
  0.0 95.9 jit_solution(9151425034139536226)
XLA Ops:
  0.6 93.9 %shard_map.131 = (bf16[64,1024]{1,0:T(8,128)(2,1)S(1)}, bf16[48,2048]{1,0:T(8,128)(2,1)S(1)}) custom-call(s32[2,768]{1,0:T(2,128)} %bitcast.20, f32[2,768]{1,0:T(2,128)} %bitcast.21, bf16[48,2048]{1,0:T(8,128)(2,1)} %x_hbm.1, f32[1,2048]{1,0:T(1,128)} %bitcast.19, bf16[64,1024]{1,0:T(8,128)(2,1)} %bitcast.18, f32[1,64]{1,0:T(1,128)} %bitcast.22, ...), custom_call_target="tpu_custom_call" | custom-call | tf_op jit(solution)/shard_map/pallas_call | solution.py:567
  94.6 0.7 copy.16
  95.2 0.7 copy.17
